TPU v7x, 32 devices: a whole 2x2x4 slice. The times are simulated.
32 devices in a mesh: kv: 8 (over z, y), tp: 4 (over x, core).
Axes of the slice: x: 2, y: 2, z: 4, core: 2. Of those that a mesh axis runs over, the one named last changes fastest.
Arguments:
- tokens: bfloat16 [64, 6, 4096], P('kv'), may hold values from -6 to 6
- norm_gain: float32 [4096], replicated, may hold values from 0.1 to 1.9
- w_query: bfloat16 [4096, 2048], P('kv', 'tp'), may hold values from -0.09375 to 0.09375
- w_key: bfloat16 [4096, 2048], P('kv', 'tp'), may hold values from -0.09375 to 0.09375
- w_value: bfloat16 [4096, 2048], P('kv', 'tp'), may hold values from -0.09375 to 0.09375
- w_outgate: bfloat16 [4096, 2048], P('kv', 'tp'), may hold values from -0.09375 to 0.09375
- w_gates: bfloat16 [4096, 2, 16], P('kv', None, 'tp'), may hold values from -0.09375 to 0.09375
- forget_bias: float32 [16], P('tp'), may hold values from 1 to 6
- head_gain: float32 [2048], P('tp'), may hold values from 0.1 to 1.9
- w_mix: bfloat16 [2048, 4096], P('tp', 'kv'), may hold values from -0.125 to 0.125
- state_cell: float32 [64, 16, 128, 128], P('kv', 'tp'), may hold values from -4 to 4
- state_norm: float32 [64, 16, 128], P('kv', 'tp'), may hold values from -4 to 4
- state_max: float32 [64, 16], P('kv', 'tp'), may hold values from -4 to 120
- pend_keys: bfloat16 [64, 6, 2048], P('kv', None, 'tp'), may hold values from -6 to 6
- pend_values: bfloat16 [64, 6, 2048], P('kv', None, 'tp'), may hold values from -6 to 6
- pend_gates: float32 [64, 6, 2, 16], P('kv', None, None, 'tp'), may hold values from -6 to 6
- accepted: int32 [64], P('kv'), may hold values from 0 to 6
Outputs:
- mixed: bfloat16 [64, 6, 4096], P('kv', None, 'tp')
- new_cell: float32 [64, 16, 128, 128], P('kv', 'tp')
- new_norm: float32 [64, 16, 128], P('kv', 'tp')
- new_max: float32 [64, 16], P('kv', 'tp')
All inputs are finite; a program needn't handle non-finite values.
Results may differ from a plain program's by a relative error of at most 0.018.
Values may be sent and summed in bfloat16 or wider, within the bound.
A program may use at most 128 MiB of HBM per device.

v0:
```python
import functools

import jax
import jax.numpy as jnp
from jax import lax
from jax.experimental import pallas as pl
from jax.experimental.pallas import tpu as pltpu
from jax.sharding import PartitionSpec as P

epsilon = 1e-06
very_low = -1e30
highest = lax.Precision.HIGHEST


def shortened(shard):

    def short(part):
        return part.astype(jnp.bfloat16) if part.dtype == jnp.float32 else part

    return jax.tree.map(short, shard)


def from_partner(shard, axis, stride):
    return lax.ppermute(shard, axis, [(i, i ^ 1 << stride) for i in range(lax.axis_size(axis))])


def running_sum(values):
    steps = values.shape[1]
    upto = jnp.arange(steps)[:, None] >= jnp.arange(steps)[None, :]
    return jnp.sum(jnp.where(upto[None, :, :, None], values[:, None], 0.0), axis=2)


def fold_pending(
    cell_state, normer, stabilizer, key_rows, value_rows, gate_rows, forget_shift, accepted
):
    proposals = key_rows.shape[1]
    accepted_mask = jnp.arange(proposals)[None, :, None] < accepted[:, None, None]
    log_in = jnp.where(accepted_mask, gate_rows[:, :, 0, :], very_low)
    log_keep = jnp.where(
        accepted_mask, jax.nn.log_sigmoid(gate_rows[:, :, 1, :] + forget_shift), 0.0
    )
    running = running_sum(log_keep)
    block_total = running[:, -1]
    log_w = block_total[:, None, :] - running + log_in
    new_max = jnp.maximum(block_total + stabilizer, jnp.max(log_w, axis=1))
    weights = jnp.exp(log_w - new_max[:, None, :])
    carried = jnp.exp(block_total + stabilizer - new_max)
    weighted_keys = weights[..., None] * key_rows
    cell_new = carried[..., None, None] * cell_state + jnp.einsum(
        "sphd,sphe->shde", weighted_keys, value_rows, precision=highest
    )
    norm_new = carried[..., None] * normer + jnp.sum(weighted_keys, axis=1)
    return (cell_new, norm_new, new_max)


def read_block(queries, key_rows, value_rows, log_in, log_keep, cell_state, normer, stabilizer):
    proposals = queries.shape[1]
    causal = jnp.arange(proposals)[:, None] >= jnp.arange(proposals)[None, :]
    running_h = jnp.moveaxis(running_sum(log_keep), 1, 2)
    input_h = jnp.moveaxis(log_in, 1, 2)
    log_d = jnp.where(
        causal, running_h[..., :, None] - running_h[..., None, :] + input_h[..., None, :], very_low
    )
    log_p = running_h + stabilizer[..., None]
    top_log = jnp.maximum(log_p, jnp.max(log_d, axis=-1))
    decays = jnp.exp(log_d - top_log[..., None])
    prior_w = jnp.exp(log_p - top_log)
    scores = jnp.einsum("sthd,suhd->shtu", queries, key_rows, precision=highest) * decays
    numerator = jnp.einsum("shtu,suhe->shte", scores, value_rows, precision=highest)
    numerator = numerator + prior_w[..., None] * jnp.einsum(
        "sthd,shde->shte", queries, cell_state, precision=highest
    )
    denominator = jnp.sum(scores, axis=-1) + prior_w * jnp.einsum(
        "sthd,shd->sht", queries, normer, precision=highest
    )
    hidden_out = numerator / jnp.maximum(jnp.abs(denominator), jnp.exp(-top_log))[..., None]
    return jnp.moveaxis(hidden_out, 1, 2)


def digit_of(own, bit):
    return own // 2**bit % 2


def collect_digits(pieces, dims, own, bits, sender):
    for bit in bits:
        others = sender(pieces, bit)
        first = digit_of(own, bit) == 0
        pieces = tuple(
            (
                jnp.where(
                    first,
                    jnp.concatenate((mine, theirs), axis=dim),
                    jnp.concatenate((theirs, mine), axis=dim),
                )
                for mine, theirs, dim in zip(pieces, others, dims)
            )
        )
    return pieces


def butterfly(blocks, own, near_bits, sender):
    for bit in range(near_bits):
        axis = near_bits - 1 - bit
        mine_digit = digit_of(own, bit)
        kept = lax.dynamic_index_in_dim(blocks, mine_digit, axis, keepdims=False)
        outgoing = lax.dynamic_index_in_dim(blocks, 1 - mine_digit, axis, keepdims=False)
        arrived = sender(outgoing, bit)
        blocks = jnp.where(
            mine_digit == 0,
            jnp.stack((kept, arrived), axis=axis),
            jnp.stack((arrived, kept), axis=axis),
        )
    return blocks


def halving(terms, own, near_bits, sender):
    for bit in range(near_bits - 1, -1, -1):
        mine_digit = digit_of(own, bit)
        kept = tuple(
            (lax.dynamic_index_in_dim(term, mine_digit, 0, keepdims=False) for term in terms)
        )
        outgoing = tuple(
            (lax.dynamic_index_in_dim(term, 1 - mine_digit, 0, keepdims=False) for term in terms)
        )
        arrived = sender(outgoing, bit)
        terms = tuple((left + right for left, right in zip(kept, arrived)))
    return terms


def greet(others):
    barrier = pltpu.get_barrier_semaphore()
    for where in others:
        pl.semaphore_signal(
            barrier, inc=1, device_id=where, device_id_type=pl.DeviceIdType.MESH
        )
    pl.semaphore_wait(barrier, len(others))


def project_kernel(
    ways,
    tok_ref,
    gain_ref,
    wq_ref,
    wk_ref,
    wv_ref,
    wo_ref,
    wg_ref,
    out_ref,
    gate_ref,
    tok_in,
    wg_in,
    pair_out,
    pair_in,
    far_out,
    far_in,
    total,
    tok_send,
    tok_recv,
    wg_send,
    wg_recv,
    pair_send,
    pair_recv,
    far_send,
    far_recv,
):
    me = lax.axis_index("kv")
    far = ways // 2
    place, side = me // 2, lax.rem(me, 2)
    rows = wq_ref.shape[0]
    width = wq_ref.shape[1]
    model_width = tok_ref.shape[1]

    def ahead(hop, other):
        return 2 * lax.rem(place + hop, far) + (1 - side if other else side)

    def behind(hop, other):
        return 2 * lax.rem(place - hop + far, far) + (1 - side if other else side)

    def columns(owner):
        return pl.ds(pl.multiple_of(owner * rows, rows), rows)

    def remote(source, target, send_sem, recv_sem, there):
        copy = pltpu.make_async_remote_copy(
            src_ref=source,
            dst_ref=target,
            send_sem=send_sem,
            recv_sem=recv_sem,
            device_id={"kv": there},
            device_id_type=pl.DeviceIdType.MESH,
        )
        copy.start()
        return copy

    hops = list(range(1, far))
    peers = [(hop, 1) for hop in hops] + [(0, 1)] + [(hop, 0) for hop in hops]
    greet([{"kv": ahead(hop, other)} for hop, other in peers])

    tok_copies, wg_copies = {}, {}
    for hop, other in peers:
        slot = 2 * hop + other
        there = ahead(hop, other)
        tok_copies[slot] = remote(
            tok_ref.at[:, columns(there)],
            tok_in.at[slot],
            tok_send.at[slot],
            tok_recv.at[slot],
            there,
        )
    for hop, other in peers:
        slot = 2 * hop + other
        wg_copies[slot] = remote(
            wg_ref, wg_in.at[slot], wg_send.at[slot], wg_recv.at[slot], ahead(hop, other)
        )

    weights = (wq_ref, wk_ref, wv_ref, wo_ref)
    spans = [slice(index * width, (index + 1) * width) for index in range(len(weights))]
    gain = gain_ref[:, columns(me)]

    def scaled(block, gain_part):
        return (block.astype(jnp.float32) * gain_part).astype(jnp.bfloat16)

    def times(block, weight):
        return jnp.dot(block, weight[...], preferred_element_type=jnp.float32)

    halves = (slice(0, 2 * width), slice(2 * width, 4 * width))
    pair_copies, far_copies = {}, {}
    for hop in hops + [0]:
        slot = 2 * hop + 1
        tok_copies[slot].wait_recv()
        block = scaled(tok_in[slot], gain)
        for half, cut in enumerate(halves):
            for index in (2 * half, 2 * half + 1):
                pair_out[hop, :, spans[index]] = times(block, weights[index]).astype(jnp.bfloat16)
            pair_copies[hop, half] = remote(
                pair_out.at[hop, :, cut],
                pair_in.at[hop, :, cut],
                pair_send.at[2 * hop + half],
                pair_recv.at[2 * hop + half],
                behind(0, 1),
            )

    own_block = scaled(tok_ref[:, columns(me)], gain)
    for span, weight in zip(spans, weights):
        total[:, span] = times(own_block, weight)
    squares = jnp.zeros((tok_ref.shape[0], 1), jnp.float32)
    for step in range(ways):
        part = tok_ref[:, step * rows : (step + 1) * rows].astype(jnp.float32)
        squares = squares + jnp.sum(part * part, axis=1, keepdims=True)
    row_scale = lax.rsqrt(squares / model_width + epsilon)

    for hop in hops:
        slot = 2 * hop
        tok_copies[slot].wait_recv()
        block = scaled(tok_in[slot], gain)
        for half, cut in enumerate(halves):
            pair_copies[hop, half].wait_recv()
            for index in (2 * half, 2 * half + 1):
                span = spans[index]
                far_out[hop, :, span] = (
                    times(block, weights[index]) + pair_in[hop, :, span].astype(jnp.float32)
                ).astype(jnp.bfloat16)
            far_copies[hop, half] = remote(
                far_out.at[hop, :, cut],
                far_in.at[hop, :, cut],
                far_send.at[2 * hop + half],
                far_recv.at[2 * hop + half],
                behind(hop, 0),
            )

    contract = (((1,), (1,)), ((), ()))
    gates = lax.dot_general(own_block, wg_ref[...], contract, preferred_element_type=jnp.float32)
    for hop, other in peers:
        slot = 2 * hop + other
        wg_copies[slot].wait_recv()
        owner = behind(hop, other)
        block = scaled(tok_ref[:, columns(owner)], gain_ref[:, columns(owner)])
        gates = gates + lax.dot_general(
            block, wg_in[slot], contract, preferred_element_type=jnp.float32
        )
    gate_ref[...] = gates * row_scale

    pair_copies[0, 0].wait_recv()
    pair_copies[0, 1].wait_recv()
    for span in spans:
        total[:, span] += pair_in[0, :, span].astype(jnp.float32)
    for hop in hops:
        far_copies[hop, 0].wait_recv()
        far_copies[hop, 1].wait_recv()
        for span in spans:
            total[:, span] += far_in[hop, :, span].astype(jnp.float32)
    for span in spans:
        out_ref[:, span] = (total[:, span] * row_scale).astype(jnp.bfloat16)
    for group in (tok_copies, wg_copies, pair_copies, far_copies):
        for copy in group.values():
            copy.wait_send()


def project(flat_rows, norm_gain, weights, w_gates):
    ways = lax.axis_size("kv")
    far = ways // 2
    count, model_width = flat_rows.shape
    rows, width = weights[0].shape
    columns = width * len(weights)
    gate_rows = w_gates.shape[1]
    vmem = pl.BlockSpec(memory_space=pltpu.VMEM)
    return pl.pallas_call(
        functools.partial(project_kernel, ways),
        out_shape=(
            jax.ShapeDtypeStruct((count, columns), jnp.bfloat16),
            jax.ShapeDtypeStruct((count, gate_rows), jnp.float32),
        ),
        in_specs=[vmem] * 7,
        out_specs=(vmem, vmem),
        scratch_shapes=[
            pltpu.VMEM((ways, count, rows), jnp.bfloat16),
            pltpu.VMEM((ways, gate_rows, rows), jnp.bfloat16),
        ]
        + [pltpu.VMEM((far, count, columns), jnp.bfloat16)] * 4
        + [pltpu.VMEM((count, columns), jnp.float32)]
        + [pltpu.SemaphoreType.DMA((ways,))] * 8,
        compiler_params=pltpu.CompilerParams(collective_id=0, has_side_effects=True),
    )(flat_rows, norm_gain[None, :], *weights, w_gates.T)


def mix_kernel(
    ways,
    groups,
    gated_ref,
    mix_ref,
    out_ref,
    gated_in,
    part_out,
    part_in,
    gated_send,
    gated_recv,
    part_send,
    part_recv,
):
    me = lax.axis_index("kv")
    group = lax.axis_index("tp")
    each = ways // groups
    width = mix_ref.shape[1]
    target = me // each
    spot = lax.rem(me, each) * groups + group
    at_home = target == group
    barrier = pltpu.get_barrier_semaphore()

    def signal(where):
        pl.semaphore_signal(
            barrier, inc=1, device_id=where, device_id_type=pl.DeviceIdType.MESH
        )

    for step in range(1, ways):
        signal({"kv": lax.rem(me + step, ways)})
    for which in range(each):
        for other in range(groups):
            sender = group * each + which

            @pl.when(jnp.logical_or(sender != me, group != other))
            def _():
                signal({"kv": sender, "tp": other})

    @pl.when(at_home)
    def _():
        pl.semaphore_wait(barrier, 2 * (ways - 1))

    @pl.when(jnp.logical_not(at_home))
    def _():
        pl.semaphore_wait(barrier, 2 * (ways - 1) + 1)

    far = ways // 2
    place, side = me // 2, lax.rem(me, 2)
    partner = 2 * place + 1 - side
    hops = list(range(1, far))

    def gather(source, slot, there):
        copy = pltpu.make_async_remote_copy(
            src_ref=source,
            dst_ref=gated_in.at[slot],
            send_sem=gated_send.at[slot],
            recv_sem=gated_recv.at[slot],
            device_id={"kv": there},
            device_id_type=pl.DeviceIdType.MESH,
        )
        copy.start()
        return copy

    gathers = {}
    for hop in hops:
        gathers[2 * hop] = gather(gated_ref, 2 * hop, 2 * lax.rem(place + hop, far) + side)
    gathers[1] = gather(gated_ref, 1, partner)

    def outgoing(step, owner):
        return pltpu.make_async_remote_copy(
            src_ref=part_out.at[step],
            dst_ref=part_in.at[spot],
            send_sem=part_send.at[step],
            recv_sem=part_recv.at[spot],
            device_id={"kv": owner, "tp": target},
            device_id_type=pl.DeviceIdType.MESH,
        )

    kept = pltpu.make_async_copy(part_out.at[0], part_in.at[spot], part_recv.at[spot])

    def mixed(block):
        return jnp.dot(block, mix_ref[...], preferred_element_type=jnp.float32).astype(
            jnp.bfloat16
        )

    part_out[0] = mixed(gated_ref[...])

    @pl.when(at_home)
    def _():
        kept.start()

    @pl.when(jnp.logical_not(at_home))
    def _():
        outgoing(0, me).start()

    copies = []

    def answer(slot, owner):
        part_out[slot] = mixed(gated_in[slot])
        copy = outgoing(slot, owner)
        copy.start()
        copies.append(copy)

    for hop in hops:
        slot = 2 * hop
        gathers[slot].wait_recv()
        gathers[slot + 1] = gather(gated_in.at[slot], slot + 1, partner)
        answer(slot, 2 * lax.rem(place - hop + far, far) + side)
    for hop in [0] + hops:
        slot = 2 * hop + 1
        gathers[slot].wait_recv()
        answer(slot, 2 * lax.rem(place - hop + far, far) + 1 - side)

    for which in range(each):
        total = None
        for other in range(groups):
            slot = which * groups + other
            pltpu.make_async_copy(part_out.at[0], part_in.at[slot], part_recv.at[slot]).wait()
            term = part_in[slot].astype(jnp.float32)
            total = term if total is None else total + term
        out_ref[:, which * width : (which + 1) * width] = total.astype(jnp.bfloat16)
    for copy in list(gathers.values()) + copies:
        copy.wait_send()

    @pl.when(jnp.logical_not(at_home))
    def _():
        outgoing(0, me).wait_send()


def mix(gated_rows, w_mix):
    ways, groups = lax.axis_size("kv"), lax.axis_size("tp")
    count, rows = gated_rows.shape
    width = w_mix.shape[1]
    vmem = pl.BlockSpec(memory_space=pltpu.VMEM)
    dma = pltpu.SemaphoreType.DMA((ways,))
    return pl.pallas_call(
        functools.partial(mix_kernel, ways, groups),
        out_shape=jax.ShapeDtypeStruct((count, ways // groups * width), jnp.bfloat16),
        in_specs=[vmem] * 2,
        out_specs=vmem,
        scratch_shapes=[
            pltpu.VMEM((ways, count, rows), jnp.bfloat16),
            pltpu.VMEM((ways, count, width), jnp.bfloat16),
            pltpu.VMEM((ways, count, width), jnp.bfloat16),
        ]
        + [dma] * 4,
        compiler_params=pltpu.CompilerParams(collective_id=1, has_side_effects=True),
    )(gated_rows, w_mix)


def project_by_digits(flat_rows, norm_gain, weights, w_mix):
    token_count, model_width = flat_rows.shape
    shard_rows = weights[0].shape[0]
    own = lax.axis_index("kv")
    kv_bits = lax.axis_size("kv").bit_length() - 1
    near_bits = kv_bits // 2
    near = 2**near_bits
    far = lax.axis_size("kv") // near
    digit_shape = (2,) * near_bits
    collected = collect_digits(
        weights + (w_mix,),
        (0, 0, 0, 0, 0, 1),
        own,
        range(near_bits, kv_bits),
        lambda parts, bit: jax.tree.map(
            lambda part, own: part.astype(own.dtype),
            from_partner(shortened(parts), "kv", bit),
            parts,
        ),
    )
    far_mix = collected[5]
    token_digits = jnp.moveaxis(flat_rows.reshape(token_count, far, near, shard_rows), 2, 0)
    token_digits = token_digits.reshape(digit_shape + (token_count, far, shard_rows))
    arrived = butterfly(
        token_digits, own, near_bits, lambda part, bit: from_partner(part, "kv", bit)
    )
    gathered = arrived.reshape(near * token_count, far * shard_rows)
    gain_part = lax.dynamic_index_in_dim(
        norm_gain.reshape(far, near, shard_rows), own % near, 1, keepdims=False
    ).reshape(far * shard_rows)
    widened = gathered.astype(jnp.float32)
    scaled_in = (widened * gain_part).astype(jnp.bfloat16)
    partials = tuple(
        (
            jnp.dot(scaled_in, weight, preferred_element_type=jnp.float32).reshape(
                digit_shape + (token_count, weight.shape[1])
            )
            for weight in collected[:5]
        )
    )
    part_squares = jnp.sum(widened * widened, axis=-1).reshape(digit_shape + (token_count,))
    summed = halving(
        partials + (part_squares,),
        own,
        near_bits,
        lambda parts, bit: jax.tree.map(
            lambda part, own: part.astype(own.dtype),
            from_partner(shortened(parts), "kv", bit),
            parts,
        ),
    )
    totals = summed[:5]
    sum_squares = summed[5]
    row_scale = lax.rsqrt(sum_squares / model_width + epsilon)[:, None]
    return (
        tuple((total * row_scale).astype(jnp.bfloat16) for total in totals[:4]),
        totals[4] * row_scale,
        far_mix,
    )


def mix_by_digits(gated_rows, far_mix, model_width):
    token_count = gated_rows.shape[0]
    shard_rows = model_width // lax.axis_size("kv")
    own = lax.axis_index("kv")
    kv_bits = lax.axis_size("kv").bit_length() - 1
    near_bits = kv_bits // 2
    near = 2**near_bits
    far = lax.axis_size("kv") // near
    digit_shape = (2,) * near_bits
    near_gated = collect_digits(
        (gated_rows,),
        (0,),
        own,
        range(near_bits),
        lambda parts, bit: jax.tree.map(
            lambda part, own: part.astype(own.dtype),
            from_partner(shortened(parts), "kv", bit),
            parts,
        ),
    )[0]
    group_part = jnp.dot(near_gated, far_mix, preferred_element_type=jnp.float32).astype(
        jnp.bfloat16
    )
    group_part = group_part.reshape(digit_shape + (token_count, far, shard_rows))
    placed = butterfly(group_part, own, near_bits, lambda part, bit: from_partner(part, "kv", bit))
    placed = placed.reshape(near, token_count, far, shard_rows).transpose(1, 2, 0, 3)
    partial_out = placed.reshape(token_count, model_width).astype(jnp.float32)
    mixed_out = lax.psum_scatter(
        partial_out.astype(jnp.bfloat16), "tp", scatter_dimension=1, tiled=True
    )
    return mixed_out


def shards(
    tokens,
    norm_gain,
    w_query,
    w_key,
    w_value,
    w_outgate,
    w_gates,
    forget_bias,
    head_gain,
    w_mix,
    state_cell,
    state_norm,
    state_max,
    pend_keys,
    pend_values,
    pend_gates,
    accepted,
):
    sequences, proposals, model_width = tokens.shape
    token_count = sequences * proposals
    local_heads = forget_bias.shape[0]
    head_size = state_cell.shape[-1]
    shard_rows = w_query.shape[0]
    weights = (w_query, w_key, w_value, w_outgate)
    flat_gates = w_gates.reshape(shard_rows, -1)
    flat_rows = tokens.reshape(token_count, model_width)
    direct = (
        shard_rows % 128 == 0
        and w_mix.shape[1] % 128 == 0
        and lax.axis_size("kv") % 2 == 0
        and lax.axis_size("kv") % lax.axis_size("tp") == 0
    )
    if direct:
        columns, gate_pre = project(flat_rows, norm_gain, weights, flat_gates)
        queries, new_keys, new_values, outgate = jnp.split(columns, len(weights), axis=1)
    else:
        projected, gate_pre, far_mix = project_by_digits(
            flat_rows, norm_gain, weights + (flat_gates,), w_mix
        )
        queries, new_keys, new_values, outgate = projected
    gate_pre = gate_pre.reshape(sequences, proposals, 2, local_heads)

    def split_heads(array):
        return array.astype(jnp.float32).reshape(sequences, proposals, local_heads, head_size)

    key_scale = head_size ** (-0.5)
    cell_new, norm_new, new_max = fold_pending(
        state_cell,
        state_norm,
        state_max,
        split_heads(pend_keys) * key_scale,
        split_heads(pend_values),
        pend_gates,
        forget_bias,
        accepted,
    )
    log_in = gate_pre[:, :, 0, :]
    log_keep = jax.nn.log_sigmoid(gate_pre[:, :, 1, :] + forget_bias)
    hidden = read_block(
        split_heads(queries),
        split_heads(new_keys) * key_scale,
        split_heads(new_values),
        log_in,
        log_keep,
        cell_new,
        norm_new,
        new_max,
    )
    normed = hidden * lax.rsqrt(jnp.mean(hidden * hidden, axis=-1, keepdims=True) + epsilon)
    normed = normed * head_gain.reshape(local_heads, head_size)
    gated_rows = (jax.nn.sigmoid(split_heads(outgate)) * normed).astype(jnp.bfloat16)
    gated_rows = gated_rows.reshape(token_count, local_heads * head_size)
    if direct:
        mixed_out = mix(gated_rows, w_mix)
    else:
        mixed_out = mix_by_digits(gated_rows, far_mix, model_width)
    return (mixed_out.reshape(sequences, proposals, -1), cell_new, norm_new, new_max)


def solution(mesh):
    return jax.shard_map(
        shards,
        mesh=mesh,
        in_specs=(
            P("kv", None, None),
            P(),
            P("kv", "tp"),
            P("kv", "tp"),
            P("kv", "tp"),
            P("kv", "tp"),
            P("kv", None, "tp"),
            P("tp"),
            P("tp"),
            P("tp", "kv"),
            P("kv", "tp", None, None),
            P("kv", "tp", None),
            P("kv", "tp"),
            P("kv", None, "tp"),
            P("kv", None, "tp"),
            P("kv", None, None, "tp"),
            P("kv"),
        ),
        out_specs=(
            P("kv", None, "tp"),
            P("kv", "tp", None, None),
            P("kv", "tp", None),
            P("kv", "tp"),
        ),
        check_vma=False,
    )
```

profile of v0, /device:TPU:0, one launch (start us, length us, event | category | flops | bytes accessed | tf_op | source)
XLA Modules:
  0.0 76.3 jit_solution(18045197387965039850)
XLA Ops:
  0.6 0.8 %copy-done = bf16[8,6,512]{2,0,1:T(8,128)(2,1)S(1)} copy-done((bf16[8,6,512]{2,0,1:T(8,128)(2,1)S(1)}, bf16[8,6,512]{2,0,1:T(8,128)(2,1)}, u32[]{:S(2)}) %copy-start) | copy-done | bytes 49176
  1.4 0.7 iota_compare_fusion
  2.1 0.1 copy.159
  2.2 0.8 copy.168
  3.0 1.3 %reshape.148 = bf16[512,8]{0,1:T(8,128)(2,1)} reshape(bf16[512,2,4]{0,2,1:T(4,128)(2,1)} %param.23) | data formatting | bytes 16384 | tf_op jit(solution)/shard_map/reshape | solution.py:594
  4.3 0.8 %convert_bitcast_fusion = f32[8,6,4,128]{3,0,2,1:T(8,128)S(1)} fusion(bf16[8,6,512]{2,0,1:T(8,128)(2,1)} %param.30), kind=kLoop, calls=%fused_computation.15 | loop fusion | flops 24576 | bytes 147456 | tf_op jit(solution)/shard_map/reshape | solution.py:613
  5.1 1.2 %copy.156 = bf16[8,6,4096]{2,1,0:T(8,128)(2,1)S(1)} copy(bf16[8,6,4096]{2,0,1:T(8,128)(2,1)} %param.17) | data formatting | bytes 786432 | tf_op args[0]
  6.4 0.9 %reshape.147.tok_ref = bf16[48,4096]{1,0:T(8,128)(2,1)} reshape(bf16[8,6,4096]{2,1,0:T(8,128)(2,1)S(1)} %copy.156) | data formatting | bytes 786432 | tf_op jit(solution)/shard_map/reshape | solution.py:595
  7.2 36.7 %shard_map.192 = (bf16[48,2048]{1,0:T(8,128)(2,1)}, f32[48,8]{1,0:T(8,128)}) custom-call(bf16[48,4096]{1,0:T(8,128)(2,1)} %reshape.147.tok_ref, f32[1,4096]{1,0:T(1,128)} %bitcast.93, bf16[512,512]{1,0:T(8,128)(2,1)} %wq_ref.1, bf16[512,512]{1,0:T(8,128)(2,1)} %wk_ref.1, bf16[512,512]{1,0:T(8,128)(2,1)} %wv_ref.1, bf16[512,512]{1,0:T(8,128)(2,1)} %wo_ref.1, ...), custom_call_target="tpu_custom_call" | custom-call | tf_op jit(solution)/shard_map/pallas_call | solution.py:306
  44.0 0.8 %copy.160 = f32[48,8]{0,1:T(8,128)S(1)} copy(f32[48,8]{1,0:T(8,128)} %get-tuple-element.7) | data formatting | bytes 3072 | tf_op jit(solution)/shard_map/pallas_call | solution.py:306
  45.0 0.1 fusion.16
  45.1 0.1 select_reduce_fusion.1
  45.6 0.2 fusion.5
  46.3 0.8 %fusion.24 = (bf16[48,512]{1,0:T(8,128)(2,1)S(1)}, bf16[48,512]{1,0:T(8,128)(2,1)S(1)}) fusion(bf16[48,2048]{1,0:T(8,128)(2,1)} %get-tuple-element.6), kind=kLoop, calls=%fused_computation.56 | loop fusion | bytes 196608 | tf_op jit(solution)/shard_map/split | solution.py:604
  47.2 0.9 %convert_multiply_fusion.1 = (f32[48,512]{1,0:T(8,128)S(1)}, f32[48,512]{1,0:T(8,128)S(1)}) fusion(bf16[48,2048]{1,0:T(8,128)(2,1)} %get-tuple-element.6), kind=kLoop, calls=%fused_computation.17 | loop fusion | flops 147456 | bytes 294912 | tf_op jit(solution)/shard_map/mul | solution.py:630
  48.1 0.3 fusion.26
  48.5 0.2 fusion.8
  49.1 3.7 %multiply_add_fusion = f32[8,4,128,128]{3,2,1,0:T(8,128)S(1)} fusion(f32[8,4,128,128]{3,2,1,0:T(8,128)} %param.27, f32[8,4]{1,0:T(8,128)S(1)} %get-tuple-element.34, f32[8,6,4,128]{3,0,2,1:T(8,128)S(1)} %convert_bitcast_fusion, bf16[8,6,4,128]{3,0,2,1:T(8,128)(2,1)S(1)} %bitcast.86, f32[8,6,4]{1,2,0:T(4,128)S(1)} %copy.179), kind=kOutput, calls=%fused_computation | convolution fusion | flops 38821888 | bytes 4342656 | tf_op jit(solution)/shard_map/sphd,sphe->shde/dot_general | solution.py:49
  52.9 1.1 %fusion.2 = f32[8,6,4,128]{3,1,2,0:T(8,128)S(1)} fusion(f32[8,4,128,128]{3,2,1,0:T(8,128)S(1)} %multiply_add_fusion, bf16[8,6,4,128]{3,2,1,0:T(4,128)(2,1)S(1)} %reshape.149, f32[8,6,4]{1,2,0:T(4,128)S(1)} %copy.178), kind=kOutput, calls=%fused_computation.6 | convolution fusion | flops 37773312 | bytes 2245376 | tf_op jit(solution)/shard_map/sthd,shde->shte/dot_general | solution.py:70
  54.0 0.4 multiply_reduce_fusion
  54.6 0.6 copy.225
  55.2 19.4 %shard_map.193 = bf16[48,1024]{1,0:T(8,128)(2,1)} custom-call(bf16[48,512]{1,0:T(8,128)(2,1)} %bitcast.89, bf16[512,512]{1,0:T(8,128)(2,1)} %mix_ref.1), custom_call_target="tpu_custom_call" | custom-call | tf_op jit(solution)/shard_map/pallas_call | solution.py:460
  74.6 0.9 %reshape.155 = bf16[8,6,1024]{2,1,0:T(8,128)(2,1)S(1)} reshape(bf16[48,1024]{1,0:T(8,128)(2,1)} %shard_map.193) | data formatting | bytes 196608 | tf_op jit(solution)/shard_map/reshape | solution.py:646
  75.6 0.7 copy.188
  (49 shorter events, 1.8 us)
Async XLA Ops:
  0.6 0.8 %copy-start = (bf16[8,6,512]{2,0,1:T(8,128)(2,1)S(1)}, bf16[8,6,512]{2,0,1:T(8,128)(2,1)}, u32[]{:S(2)}) copy-start(bf16[8,6,512]{2,0,1:T(8,128)(2,1)} %param.31) | copy-start | bytes 147460
  5.1 39.9 %copy-start.3 = (f32[8,6,2,4]{0,3,2,1:T(4,128)S(1)}, f32[8,6,2,4]{0,3,2,1:T(4,128)}, u32[]{:S(2)}) copy-start(f32[8,6,2,4]{0,3,2,1:T(4,128)} %param.32) | copy-start | bytes 4612
  5.1 39.9 %copy-start.8 = (f32[4]{0:T(128)S(1)}, f32[4]{0:T(128)}, u32[]{:S(2)}) copy-start(f32[4]{0:T(128)} %param.24) | copy-start | bytes 52
  6.3 39.7 %copy-start.2 = (bf16[8,6,512]{2,0,1:T(8,128)(2,1)S(1)}, bf16[8,6,512]{2,0,1:T(8,128)(2,1)}, u32[]{:S(2)}) copy-start(bf16[8,6,512]{2,0,1:T(8,128)(2,1)} %param.30) | copy-start | bytes 147460
  6.3 39.8 %copy-start.5 = (f32[8,4,128]{2,1,0:T(4,128)S(1)}, f32[8,4,128]{2,1,0:T(4,128)}, u32[]{:S(2)}) copy-start(f32[8,4,128]{2,1,0:T(4,128)} %param.28) | copy-start | bytes 49156
  45.5 7.4 %copy-start.4 = (f32[8,4]{0,1:T(4,128)}, f32[8,4]{0,1:T(4,128)S(1)}, u32[]{:S(2)}) copy-start(f32[8,4]{0,1:T(4,128)S(1)} %copy.171) | copy-start | bytes 388
  46.2 6.6 %copy-start.6 = (f32[8,4,128]{2,1,0:T(4,128)}, f32[8,4,128]{2,1,0:T(4,128)S(1)}, u32[]{:S(2)}) copy-start(f32[8,4,128]{2,1,0:T(4,128)S(1)} %multiply_add_fusion.1) | copy-start | bytes 49156
  52.9 21.8 %copy-start.1 = (f32[8,4,128,128]{3,2,1,0:T(8,128)}, f32[8,4,128,128]{3,2,1,0:T(8,128)S(1)}, u32[]{:S(2)}) copy-start(f32[8,4,128,128]{3,2,1,0:T(8,128)S(1)} %multiply_add_fusion) | copy-start | bytes 6291460
  52.9 1.5 %copy-start.7 = (f32[512]{0:T(512)S(1)}, f32[512]{0:T(512)}, u32[]{:S(2)}) copy-start(f32[512]{0:T(512)} %param.25) | copy-start | bytes 6148
where the time goes:
time: 76.9 us; the launch traced here: 76.3 us
  Pallas kernels  56.1 us (73%)
  local copies, waits for them, and re-layouts  10.4 us (14%)
  matrix products  5.73 us (7%)
  other arithmetic  3.09 us (4%)
  between operations  0.88 us (1%)
    pallas_call x1, Pallas kernels, project(): pl.pallas_call(functools.partial(project_kernel, ways), out_shape=(jax.Sh...  36.7 us
    pallas_call x1, Pallas kernels, mix(): pl.pallas_call(functools.partial(mix_kernel, ways, groups), out_shape=jax...  19.4 us
    unnamed x24, local copies, waits for them, and re-layouts  4.34 us
    dot_general x1, matrix products, fold_pending(): jnp.einsum('sphd,sphe->shde', weighted_keys, value_rows, precision=highest)  3.7 us

commit v1 on v0

v1 whole, which is shorter than its diff:
```python
import functools

import jax
import jax.numpy as jnp
from jax import lax
from jax.experimental import pallas as pl
from jax.experimental.pallas import tpu as pltpu
from jax.sharding import PartitionSpec as P

epsilon = 1e-06
very_low = -1e30
highest = lax.Precision.HIGHEST


def shortened(shard):

    def short(part):
        return part.astype(jnp.bfloat16) if part.dtype == jnp.float32 else part

    return jax.tree.map(short, shard)


def from_partner(shard, axis, stride):
    return lax.ppermute(shard, axis, [(i, i ^ 1 << stride) for i in range(lax.axis_size(axis))])


def running_sum(values):
    steps = values.shape[1]
    upto = jnp.arange(steps)[:, None] >= jnp.arange(steps)[None, :]
    return jnp.sum(jnp.where(upto[None, :, :, None], values[:, None], 0.0), axis=2)


def fold_pending(
    cell_state, normer, stabilizer, key_rows, value_rows, gate_rows, forget_shift, accepted
):
    proposals = key_rows.shape[1]
    accepted_mask = jnp.arange(proposals)[None, :, None] < accepted[:, None, None]
    log_in = jnp.where(accepted_mask, gate_rows[:, :, 0, :], very_low)
    log_keep = jnp.where(
        accepted_mask, jax.nn.log_sigmoid(gate_rows[:, :, 1, :] + forget_shift), 0.0
    )
    running = running_sum(log_keep)
    block_total = running[:, -1]
    log_w = block_total[:, None, :] - running + log_in
    new_max = jnp.maximum(block_total + stabilizer, jnp.max(log_w, axis=1))
    weights = jnp.exp(log_w - new_max[:, None, :])
    carried = jnp.exp(block_total + stabilizer - new_max)
    weighted_keys = weights[..., None] * key_rows
    cell_new = carried[..., None, None] * cell_state + jnp.einsum(
        "sphd,sphe->shde", weighted_keys, value_rows, precision=highest
    )
    norm_new = carried[..., None] * normer + jnp.sum(weighted_keys, axis=1)
    return (cell_new, norm_new, new_max)


def read_block(queries, key_rows, value_rows, log_in, log_keep, cell_state, normer, stabilizer):
    proposals = queries.shape[1]
    causal = jnp.arange(proposals)[:, None] >= jnp.arange(proposals)[None, :]
    running_h = jnp.moveaxis(running_sum(log_keep), 1, 2)
    input_h = jnp.moveaxis(log_in, 1, 2)
    log_d = jnp.where(
        causal, running_h[..., :, None] - running_h[..., None, :] + input_h[..., None, :], very_low
    )
    log_p = running_h + stabilizer[..., None]
    top_log = jnp.maximum(log_p, jnp.max(log_d, axis=-1))
    decays = jnp.exp(log_d - top_log[..., None])
    prior_w = jnp.exp(log_p - top_log)
    scores = jnp.einsum("sthd,suhd->shtu", queries, key_rows, precision=highest) * decays
    numerator = jnp.einsum("shtu,suhe->shte", scores, value_rows, precision=highest)
    numerator = numerator + prior_w[..., None] * jnp.einsum(
        "sthd,shde->shte", queries, cell_state, precision=highest
    )
    denominator = jnp.sum(scores, axis=-1) + prior_w * jnp.einsum(
        "sthd,shd->sht", queries, normer, precision=highest
    )
    hidden_out = numerator / jnp.maximum(jnp.abs(denominator), jnp.exp(-top_log))[..., None]
    return jnp.moveaxis(hidden_out, 1, 2)


def digit_of(own, bit):
    return own // 2**bit % 2


def collect_digits(pieces, dims, own, bits, sender):
    for bit in bits:
        others = sender(pieces, bit)
        first = digit_of(own, bit) == 0
        pieces = tuple(
            (
                jnp.where(
                    first,
                    jnp.concatenate((mine, theirs), axis=dim),
                    jnp.concatenate((theirs, mine), axis=dim),
                )
                for mine, theirs, dim in zip(pieces, others, dims)
            )
        )
    return pieces


def butterfly(blocks, own, near_bits, sender):
    for bit in range(near_bits):
        axis = near_bits - 1 - bit
        mine_digit = digit_of(own, bit)
        kept = lax.dynamic_index_in_dim(blocks, mine_digit, axis, keepdims=False)
        outgoing = lax.dynamic_index_in_dim(blocks, 1 - mine_digit, axis, keepdims=False)
        arrived = sender(outgoing, bit)
        blocks = jnp.where(
            mine_digit == 0,
            jnp.stack((kept, arrived), axis=axis),
            jnp.stack((arrived, kept), axis=axis),
        )
    return blocks


def halving(terms, own, near_bits, sender):
    for bit in range(near_bits - 1, -1, -1):
        mine_digit = digit_of(own, bit)
        kept = tuple(
            (lax.dynamic_index_in_dim(term, mine_digit, 0, keepdims=False) for term in terms)
        )
        outgoing = tuple(
            (lax.dynamic_index_in_dim(term, 1 - mine_digit, 0, keepdims=False) for term in terms)
        )
        arrived = sender(outgoing, bit)
        terms = tuple((left + right for left, right in zip(kept, arrived)))
    return terms


def log_sigmoid(values):
    return jnp.minimum(values, 0.0) - jnp.log1p(jnp.exp(-jnp.abs(values)))


def flipped(index, bits):
    place = 1
    while place <= bits:
        if bits // place % 2:
            index = index + place * (1 - 2 * (index // place % 2))
        place *= 2
    return index


def step_kernel(
    ways,
    groups,
    seqs,
    tok_hbm,
    gain_hbm,
    wq_hbm,
    wk_hbm,
    wv_hbm,
    wo_hbm,
    wg_hbm,
    bias_hbm,
    head_gain_hbm,
    mix_hbm,
    cell_hbm,
    norm_hbm,
    max_hbm,
    pend_k_hbm,
    pend_v_hbm,
    pend_g_hbm,
    accepted_hbm,
    out_hbm,
    cell_out_hbm,
    norm_out_hbm,
    max_out_hbm,
    tok,
    gain,
    weights,
    wg,
    bias,
    head_gain,
    mix_w,
    cell,
    norm,
    stab,
    pend_k,
    pend_v,
    pend_g,
    accepted,
    out,
    cell_new,
    norm_new,
    max_new,
    tok_in,
    scaled,
    wg_in,
    sums,
    part_out,
    part_in,
    fold_rows,
    cell_high,
    cell_low,
    norm_head,
    decay,
    scale_col,
    gated,
    gated_in,
    swap_out,
    swap_in,
    kept,
    answer_out,
    answer_in,
    load_sem,
    store_sem,
    tok_send,
    tok_recv,
    fwd_send,
    fwd_recv,
    wg_send,
    wg_recv,
    part_send,
    part_recv,
    gated_send,
    gated_recv,
    swap_send,
    swap_recv,
    answer_send,
    answer_recv,
):
    me = lax.axis_index("kv")
    group = lax.axis_index("tp")
    across, core = group // 2, lax.rem(group, 2)
    side = lax.rem(me, 2)
    count, model_width = tok.shape
    rows = model_width // ways
    half = rows // 2
    chunks, span = weights.shape[0], weights.shape[2] // 4
    heads, head_size = norm.shape[1], norm.shape[2]
    per_chunk = heads // chunks
    proposals = count // seqs
    bits = ways.bit_length() - 1
    f32, bf16 = jnp.float32, jnp.bfloat16
    orders = [tuple(range(bits))] * chunks

    loads = {}

    def load(name, source, target):
        copy = pltpu.make_async_copy(source, target, load_sem.at[len(loads)])
        copy.start()
        loads[name] = copy

    load("tok", tok_hbm, tok)
    load("gain", gain_hbm, gain)
    for chunk in range(chunks):
        for index, source in enumerate((wq_hbm, wk_hbm, wv_hbm, wo_hbm)):
            load(
                ("weight", chunk, index),
                source.at[:, chunk * span : (chunk + 1) * span],
                weights.at[chunk, :, index * span : (index + 1) * span],
            )
    load("wg", wg_hbm, wg)
    load("bias", bias_hbm, bias)
    load("max", max_hbm, stab)
    load("pend_g", pend_g_hbm, pend_g)
    load("accepted", accepted_hbm, accepted)
    load("pend_k", pend_k_hbm, pend_k)
    load("pend_v", pend_v_hbm, pend_v)
    load("norm", norm_hbm, norm)
    load("cell", cell_hbm, cell)
    load("head_gain", head_gain_hbm, head_gain)
    load("mix", mix_hbm, mix_w)

    target = me // 2
    at_home = jnp.logical_and(target == group, core == 0)
    barrier = pltpu.get_barrier_semaphore()

    def signal(where):
        pl.semaphore_signal(
            barrier, inc=1, device_id=where, device_id_type=pl.DeviceIdType.MESH
        )

    partner = {"tp": 2 * across + 1 - core}
    for shift in range(1, ways):
        signal({"kv": flipped(me, shift)})
    signal(partner)
    for which in range(2):
        sender = 2 * group + which
        sender_core = side + which - 2 * side * which
        for other in range(groups // 2):
            sender_group = 2 * other + sender_core

            @pl.when(jnp.logical_or(sender != me, sender_group != group))
            def _():
                signal({"kv": sender, "tp": sender_group})

    @pl.when(at_home)
    def _():
        pl.semaphore_wait(barrier, ways + ways // 2 - 1)

    @pl.when(jnp.logical_not(at_home))
    def _():
        pl.semaphore_wait(barrier, ways + ways // 2)

    sends = []

    def remote(source, target_ref, send_sem, recv_sem, where):
        copy = pltpu.make_async_remote_copy(
            src_ref=source,
            dst_ref=target_ref,
            send_sem=send_sem,
            recv_sem=recv_sem,
            device_id=where,
            device_id_type=pl.DeviceIdType.MESH,
        )
        copy.start()
        sends.append(copy)
        return copy

    def columns(owner):
        return pl.ds(pl.multiple_of(owner * rows, rows), rows)

    halves = pl.ds(pl.multiple_of(core * half, half), half)

    tok_copies, fwd_copies, wg_copies = {}, {}, {}
    loads["tok"].wait()
    whole_first = 1

    def send_tokens(shift):
        there = flipped(me, shift)
        if shift == whole_first:
            source, place = tok.at[:, columns(there)], tok_in.at[shift]
        else:
            source = tok.at[:, pl.ds(pl.multiple_of(there * rows + core * half, half), half)]
            place = tok_in.at[shift, :, halves]
        tok_copies[shift] = remote(
            source, place, tok_send.at[shift], tok_recv.at[shift], {"kv": there}
        )

    first_sends = [shift for shift in range(ways - 1, 1, -1) if shift % 2]
    keepers = [shift for shift in range(ways - 1, 0, -1) if not shift % 2]
    for shift in [whole_first] + first_sends + keepers:
        send_tokens(shift)
    loads["wg"].wait()
    for shift in range(1, ways):
        wg_copies[shift] = remote(
            wg, wg_in.at[shift], wg_send.at[shift], wg_recv.at[shift], {"kv": flipped(me, shift)}
        )

    loads["gain"].wait()
    own_gain = gain[:, columns(me)]

    def scale_block(shift, block):
        scaled[shift] = (block.astype(f32) * own_gain).astype(bf16)

    def forward(shift):
        tok_copies[shift].wait_recv()
        place = tok_in.at[shift, :, halves]
        fwd_copies[shift] = remote(
            place, place, fwd_send.at[shift], fwd_recv.at[shift], partner
        )

    def arrive(shift):
        if shift == whole_first:
            tok_copies[shift].wait_recv()
        else:
            fwd_copies[shift].wait_recv()
        scale_block(shift, tok_in[shift])

    def product(chunk, shift):
        return jnp.dot(scaled[shift], weights[chunk], preferred_element_type=f32)

    part_copies = {}

    def send_part(chunk, shift, bit, value):
        part_out[chunk, shift] = value.astype(bf16)
        part_copies[chunk, shift] = remote(
            part_out.at[chunk, shift],
            part_in.at[chunk, shift],
            part_send.at[chunk, shift],
            part_recv.at[chunk, shift],
            {"kv": flipped(me, 1 << bit)},
        )

    def first_send(chunk, shift):
        send_part(chunk, shift, orders[chunk][0], product(chunk, shift))

    scale_block(0, tok[:, columns(me)])
    squares = jnp.zeros((count, 1), f32)
    for step in range(ways):
        part = tok[:, step * rows : (step + 1) * rows].astype(f32)
        squares = squares + jnp.sum(part * part, axis=1, keepdims=True)
    row_scale = lax.rsqrt(squares / model_width + epsilon)
    scale_col[...] = jnp.broadcast_to(row_scale, scale_col.shape)

    for chunk in range(chunks):
        for index in range(4):
            loads["weight", chunk, index].wait()

    arrive(whole_first)
    for chunk in range(chunks):
        first_send(chunk, whole_first)
    for shift in first_sends:
        forward(shift)

    def eye(size):
        across_rows = lax.broadcasted_iota(jnp.int32, (size, size), 0)
        return across_rows == lax.broadcasted_iota(jnp.int32, (size, size), 1)

    def fold_gates():
        for name in ("bias", "max", "pend_g", "accepted"):
            loads[name].wait()
        bias_col = jnp.sum(
            jnp.where(eye(heads), jnp.broadcast_to(bias[...], (heads, heads)), 0.0),
            axis=1,
            keepdims=True,
        )
        log_in, running = [], []
        total = jnp.zeros((heads, seqs), f32)
        for step in range(proposals):
            taken = jnp.broadcast_to(step < accepted[...], (heads, seqs))
            log_in.append(jnp.where(taken, pend_g[step, 0], very_low))
            total = total + jnp.where(taken, log_sigmoid(pend_g[step, 1] + bias_col), 0.0)
            running.append(total)
        log_w = [total - at + ins for at, ins in zip(running, log_in)]
        carried_log = total + stab[...]
        top = carried_log
        for values in log_w:
            top = jnp.maximum(top, values)
        max_new[...] = top
        fold_rows[...] = jnp.zeros(fold_rows.shape, f32)
        pieces = [jnp.exp(values - top) for values in log_w]
        pieces = pieces + [jnp.exp(carried_log - top), top]
        for index, piece in enumerate(pieces):
            fold_rows[index * heads : (index + 1) * heads, 0:seqs] = piece
        return fold_rows[...].T[:seqs]

    stores = []

    def store(source, target_ref):
        copy = pltpu.make_async_copy(source, target_ref, store_sem.at[len(stores)])
        copy.start()
        stores.append(copy)

    key_scale = head_size ** (-0.5)

    def fold_head(cols, head):
        lanes = slice(head * head_size, (head + 1) * head_size)
        keys = pend_k[:, lanes].astype(f32)
        weighted = []
        carried = jnp.broadcast_to(
            cols[:, proposals * heads + head : proposals * heads + head + 1], (seqs, head_size)
        )
        key_sum = carried * norm[:, head, :]
        for step in range(proposals):
            weight = cols[:, step * heads + head : step * heads + head + 1]
            rows_at = keys[step * seqs : (step + 1) * seqs] * key_scale * weight
            weighted.append(rows_at)
            key_sum = key_sum + rows_at
        norm_head[head] = key_sum
        norm_new[:, head, :] = key_sum
        padding = jnp.zeros((head_size - count, head_size), f32)
        turned = jnp.concatenate(weighted + [padding], axis=0).T
        value_rows = jnp.concatenate(
            [pend_v[:, lanes].astype(f32), padding], axis=0
        ).astype(bf16)
        value_rows = jnp.concatenate([value_rows, value_rows], axis=0)
        high = turned.astype(bf16).astype(f32)
        low = turned - high
        lane = lax.rem(lax.broadcasted_iota(jnp.int32, turned.shape, 1), seqs)
        for seq in range(seqs):
            mine = lane == seq
            left = jnp.concatenate(
                [jnp.where(mine, high, 0.0).astype(bf16), jnp.where(mine, low, 0.0).astype(bf16)],
                axis=1,
            )
            update = jnp.dot(left, value_rows, preferred_element_type=f32)
            result = carried[seq : seq + 1] * cell[seq, head] + update
            cell_new[seq, head] = result
            upper = result.astype(bf16)
            at = slice(seq * head_size, (seq + 1) * head_size)
            cell_high[head, at, :] = upper
            cell_low[head, at, :] = (result - upper.astype(f32)).astype(bf16)

    cols = fold_gates()
    for shift in first_sends:
        arrive(shift)
    for chunk in range(chunks):
        for shift in first_sends:
            first_send(chunk, shift)
    for shift in keepers:
        forward(shift)
    for name in ("pend_k", "pend_v", "norm", "cell"):
        loads[name].wait()
    for head in range(heads):
        fold_head(cols, head)
    store(cell_new, cell_out_hbm)
    store(norm_new, norm_out_hbm)
    store(max_new, max_out_hbm)

    for shift in keepers:
        arrive(shift)
    for chunk in range(chunks):
        for shift in keepers + [0]:
            sums[chunk, shift // 2] = product(chunk, shift)

    contract = (((1,), (1,)), ((), ()))
    gates = [jnp.zeros((count, heads), f32)] * 2
    for shift in range(ways):
        owner = flipped(me, shift)
        if shift:
            wg_copies[shift].wait_recv()
            block = (tok[:, columns(owner)].astype(f32) * gain[:, columns(owner)]).astype(bf16)
        else:
            block = scaled[0]
        for part in range(2):
            right = wg_in[shift, part] if shift else wg[part]
            gates[part] = gates[part] + lax.dot_general(
                block, right, contract, preferred_element_type=f32
            )

    def read_gates():
        stabilizer = cols[:, (proposals + 1) * heads : (proposals + 2) * heads]
        log_in, running = [], []
        total = jnp.zeros((seqs, heads), f32)
        scale = scale_col[:, :1]
        gate_in, gate_keep = gates[0] * scale, gates[1] * scale
        index = 0
        for step in range(proposals):
            at = slice(step * seqs, (step + 1) * seqs)
            log_in.append(gate_in[at])
            total = total + log_sigmoid(gate_keep[at] + bias[...])
            running.append(total)
            log_p = total + stabilizer
            log_d = [total - running[past] + log_in[past] for past in range(step + 1)]
            top = log_p
            for values in log_d:
                top = jnp.maximum(top, values)
            for values in log_d + [log_p, None]:
                decay[index, :, :heads] = jnp.exp(-top if values is None else values - top)
                index += 1

    read_gates()

    gated_copies = {}

    def send_gated(chunk, shift, there):
        place = slice(chunk * span, (chunk + 1) * span)
        source = gated.at[:, place]
        gated_copies[chunk, shift] = remote(
            source,
            gated_in.at[shift, :, place],
            gated_send.at[chunk, shift],
            gated_recv.at[chunk, shift],
            {"kv": there},
        )

    def forward_gated(chunk, shift):
        place = slice(chunk * span, (chunk + 1) * span)
        gated_copies[chunk, shift].wait_recv()
        gated_copies[chunk, shift + 1] = remote(
            gated_in.at[shift, :, place],
            gated_in.at[shift + 1, :, place],
            gated_send.at[chunk, shift + 1],
            gated_recv.at[chunk, shift + 1],
            {"kv": flipped(me, 1)},
        )

    def read_head(chunk, local, flat):
        head = chunk * per_chunk + local
        scale = scale_col[...]

        def piece(index):
            at = index * span + local * head_size
            return (flat[:, at : at + head_size] * scale).astype(bf16).astype(f32)

        query, key, value, outgate = (piece(index) for index in range(4))
        key = key * key_scale
        sequence = lax.rem(lax.broadcasted_iota(jnp.int32, query.shape, 0), seqs)
        spread = jnp.concatenate(
            [jnp.where(sequence == seq, query, 0.0).astype(bf16) for seq in range(seqs)], axis=1
        )
        prior = jnp.dot(spread, cell_high[head], preferred_element_type=f32)
        prior = prior + jnp.dot(spread, cell_low[head], preferred_element_type=f32)
        normer = norm_head[head]
        hidden = []
        index = 0
        for step in range(proposals):
            at = slice(step * seqs, (step + 1) * seqs)
            now = query[at]
            numerator, denominator = None, None

            def factor(which):
                return decay[which, :, head : head + 1]

            for past in range(step + 1):
                before = slice(past * seqs, (past + 1) * seqs)
                score = jnp.sum(now * key[before], axis=1, keepdims=True) * factor(index + past)
                term = score * value[before]
                numerator = term if numerator is None else numerator + term
                denominator = score if denominator is None else denominator + score
            prior_w = factor(index + step + 1)
            numerator = numerator + prior_w * prior[at]
            denominator = denominator + prior_w * jnp.sum(now * normer, axis=1, keepdims=True)
            floor = factor(index + step + 2)
            hidden.append(numerator / jnp.maximum(jnp.abs(denominator), floor))
            index += step + 3
        hidden = jnp.concatenate(hidden, axis=0)
        normed = hidden * lax.rsqrt(jnp.mean(hidden * hidden, axis=1, keepdims=True) + epsilon)
        lanes = slice(head * head_size, (head + 1) * head_size)
        normed = normed * head_gain[:, lanes]
        gated[:, lanes] = (jax.nn.sigmoid(outgate) * normed).astype(bf16)

    def take(chunk, stage):
        bit = 1 << orders[chunk][stage]
        done = sum(1 << orders[chunk][early] for early in range(stage + 1))
        later = [1 << b for b in orders[chunk][stage + 1 :]]
        places = [shift for shift in range(ways) if not shift & done]
        places.sort(key=lambda shift: tuple(-(shift // b % 2) for b in later))
        for shift in places:
            part_copies[chunk, shift + bit].wait_recv()
            value = sums[chunk, shift // 2] + part_in[chunk, shift + bit].astype(f32)
            if stage + 1 < bits and shift & later[0]:
                send_part(chunk, shift, orders[chunk][stage + 1], value)
            elif stage + 1 < bits:
                sums[chunk, shift // 2] = value
            else:
                for local in range(per_chunk):
                    read_head(chunk, local, value)

    loads["head_gain"].wait()
    loads["mix"].wait()
    last = chunks - 1
    for tick in range(chunks + bits):
        for stage in range(bits):
            chunk = tick - stage
            if 0 <= chunk < chunks:
                take(chunk, stage)
                if stage == bits - 1:
                    for shift in range(ways - 1, 0, -1):
                        if chunk == last or shift == 1 or not shift % 2:
                            send_gated(chunk, shift, flipped(me, shift))
        chunk = tick - bits
        if 0 <= chunk < last:
            for shift in range(ways - 2, 0, -2):
                forward_gated(chunk, shift)

    def mixed(block):
        return jnp.dot(block, mix_w[...], preferred_element_type=f32)

    swap_copies = {}
    first_core = core == 0
    pairs = list(range(ways // 2 - 1, -1, -1))
    for pair in pairs:
        values = []
        for shift in (2 * pair, 2 * pair + 1):
            if shift:
                for chunk in range(chunks):
                    gated_copies[chunk, shift].wait_recv() if (
                        chunk == last or shift % 2
                    ) else None
                values.append(mixed(gated_in[shift]))
            else:
                values.append(mixed(gated[...]))
        kept[pair] = jnp.where(first_core, values[0], values[1]).astype(bf16)
        swap_out[pair] = jnp.where(first_core, values[1], values[0]).astype(bf16)
        swap_copies[pair] = remote(
            swap_out.at[pair], swap_in.at[pair], swap_send.at[pair], swap_recv.at[pair], partner
        )

    spot = side * (groups // 2) + across

    def answer(pair):
        base = flipped(me, 2 * pair)
        owner = base + core * (1 - 2 * side)
        return pltpu.make_async_remote_copy(
            src_ref=answer_out.at[pair],
            dst_ref=answer_in.at[spot],
            send_sem=answer_send.at[pair],
            recv_sem=answer_recv.at[spot],
            device_id={"kv": owner, "tp": target},
            device_id_type=pl.DeviceIdType.MESH,
        )

    at_own = pltpu.make_async_copy(answer_out.at[0], answer_in.at[spot], answer_recv.at[spot])
    for pair in pairs:
        swap_copies[pair].wait_recv()
        answer_out[pair] = (kept[pair].astype(f32) + swap_in[pair].astype(f32)).astype(bf16)
        if pair:
            copy = answer(pair)
            copy.start()
            sends.append(copy)
        else:

            @pl.when(at_home)
            def _():
                at_own.start()

            @pl.when(jnp.logical_not(at_home))
            def _():
                answer(0).start()

    width = mix_w.shape[1]
    for which in range(2):
        total = None
        for other in range(groups // 2):
            slot = which * (groups // 2) + other
            pltpu.make_async_copy(
                answer_out.at[0], answer_in.at[slot], answer_recv.at[slot]
            ).wait()
            term = answer_in[slot].astype(f32)
            total = term if total is None else total + term
        out[:, which * width : (which + 1) * width] = total.astype(bf16)
    store(out, out_hbm)
    for copy in sends:
        copy.wait_send()

    @pl.when(jnp.logical_not(at_home))
    def _():
        answer(0).wait_send()

    for copy in stores:
        copy.wait()


def one_step(
    tokens,
    norm_gain,
    weights,
    w_gates,
    forget_bias,
    head_gain,
    w_mix,
    state_cell,
    state_norm,
    state_max,
    pend_keys,
    pend_values,
    pend_gates,
    accepted,
):
    ways, groups = lax.axis_size("kv"), lax.axis_size("tp")
    seqs, proposals, model_width = tokens.shape
    count = seqs * proposals
    rows, width = weights[0].shape
    heads, head_size = state_norm.shape[1:]
    chunks = heads
    span = width // chunks
    f32, bf16 = jnp.float32, jnp.bfloat16

    def by_proposal(array):
        return array.transpose(1, 0, 2).reshape(count, array.shape[2])

    operands = (
        by_proposal(tokens),
        norm_gain[None, :],
        *weights,
        w_gates.transpose(1, 2, 0),
        forget_bias[None, :],
        head_gain[None, :],
        w_mix,
        state_cell,
        state_norm,
        state_max.T,
        by_proposal(pend_keys),
        by_proposal(pend_values),
        pend_gates.transpose(1, 2, 3, 0),
        accepted[None, :],
    )
    out_shape = (
        jax.ShapeDtypeStruct((count, ways // groups * width), bf16),
        jax.ShapeDtypeStruct(state_cell.shape, f32),
        jax.ShapeDtypeStruct(state_norm.shape, f32),
        jax.ShapeDtypeStruct((heads, seqs), f32),
    )
    held = [jax.ShapeDtypeStruct(array.shape, array.dtype) for array in operands]
    held = held[:2] + [jax.ShapeDtypeStruct((chunks, rows, 4 * span), bf16)] + held[6:]
    held = held + list(out_shape)
    block = (ways, count, rows)
    scratch = [pltpu.VMEM(array.shape, array.dtype) for array in held]
    scratch += [
        pltpu.VMEM(block, bf16),
        pltpu.VMEM(block, bf16),
        pltpu.VMEM((ways, 2, heads, rows), bf16),
        pltpu.VMEM((chunks, ways // 2, count, 4 * span), f32),
        pltpu.VMEM((chunks, ways, count, 4 * span), bf16),
        pltpu.VMEM((chunks, ways, count, 4 * span), bf16),
        pltpu.VMEM(((proposals + 2) * heads, 128), f32),
        pltpu.VMEM((heads, seqs * head_size, head_size), bf16),
        pltpu.VMEM((heads, seqs * head_size, head_size), bf16),
        pltpu.VMEM((heads, seqs, head_size), f32),
        pltpu.VMEM((proposals * (proposals + 5) // 2, seqs, 128), f32),
        pltpu.VMEM((count, head_size), f32),
        pltpu.VMEM((count, width), bf16),
        pltpu.VMEM((ways, count, width), bf16),
    ]
    scratch += [pltpu.VMEM((ways // 2, count, width), bf16)] * 5
    dma = pltpu.SemaphoreType.DMA
    scratch += [dma((len(operands) + 4 * chunks,)), dma((8,))]
    scratch += [dma((ways,))] * 6
    scratch += [dma((chunks, ways))] * 4
    scratch += [dma((ways,))] * 4
    anywhere = pl.BlockSpec(memory_space=pl.ANY)
    mixed_out, cell_new, norm_new, max_new = pl.pallas_call(
        functools.partial(step_kernel, ways, groups, seqs),
        out_shape=out_shape,
        in_specs=[anywhere] * len(operands),
        out_specs=(anywhere,) * 4,
        scratch_shapes=scratch,
        compiler_params=pltpu.CompilerParams(collective_id=0, has_side_effects=True),
    )(*operands)
    mixed_out = mixed_out.reshape(proposals, seqs, -1).transpose(1, 0, 2)
    return mixed_out, cell_new, norm_new, max_new.T


def project_by_digits(flat_rows, norm_gain, weights, w_mix):
    token_count, model_width = flat_rows.shape
    shard_rows = weights[0].shape[0]
    own = lax.axis_index("kv")
    kv_bits = lax.axis_size("kv").bit_length() - 1
    near_bits = kv_bits // 2
    near = 2**near_bits
    far = lax.axis_size("kv") // near
    digit_shape = (2,) * near_bits
    collected = collect_digits(
        weights + (w_mix,),
        (0, 0, 0, 0, 0, 1),
        own,
        range(near_bits, kv_bits),
        lambda parts, bit: jax.tree.map(
            lambda part, own: part.astype(own.dtype),
            from_partner(shortened(parts), "kv", bit),
            parts,
        ),
    )
    far_mix = collected[5]
    token_digits = jnp.moveaxis(flat_rows.reshape(token_count, far, near, shard_rows), 2, 0)
    token_digits = token_digits.reshape(digit_shape + (token_count, far, shard_rows))
    arrived = butterfly(
        token_digits, own, near_bits, lambda part, bit: from_partner(part, "kv", bit)
    )
    gathered = arrived.reshape(near * token_count, far * shard_rows)
    gain_part = lax.dynamic_index_in_dim(
        norm_gain.reshape(far, near, shard_rows), own % near, 1, keepdims=False
    ).reshape(far * shard_rows)
    widened = gathered.astype(jnp.float32)
    scaled_in = (widened * gain_part).astype(jnp.bfloat16)
    partials = tuple(
        (
            jnp.dot(scaled_in, weight, preferred_element_type=jnp.float32).reshape(
                digit_shape + (token_count, weight.shape[1])
            )
            for weight in collected[:5]
        )
    )
    part_squares = jnp.sum(widened * widened, axis=-1).reshape(digit_shape + (token_count,))
    summed = halving(
        partials + (part_squares,),
        own,
        near_bits,
        lambda parts, bit: jax.tree.map(
            lambda part, own: part.astype(own.dtype),
            from_partner(shortened(parts), "kv", bit),
            parts,
        ),
    )
    totals = summed[:5]
    sum_squares = summed[5]
    row_scale = lax.rsqrt(sum_squares / model_width + epsilon)[:, None]
    return (
        tuple((total * row_scale).astype(jnp.bfloat16) for total in totals[:4]),
        totals[4] * row_scale,
        far_mix,
    )


def mix_by_digits(gated_rows, far_mix, model_width):
    token_count = gated_rows.shape[0]
    shard_rows = model_width // lax.axis_size("kv")
    own = lax.axis_index("kv")
    kv_bits = lax.axis_size("kv").bit_length() - 1
    near_bits = kv_bits // 2
    near = 2**near_bits
    far = lax.axis_size("kv") // near
    digit_shape = (2,) * near_bits
    near_gated = collect_digits(
        (gated_rows,),
        (0,),
        own,
        range(near_bits),
        lambda parts, bit: jax.tree.map(
            lambda part, own: part.astype(own.dtype),
            from_partner(shortened(parts), "kv", bit),
            parts,
        ),
    )[0]
    group_part = jnp.dot(near_gated, far_mix, preferred_element_type=jnp.float32).astype(
        jnp.bfloat16
    )
    group_part = group_part.reshape(digit_shape + (token_count, far, shard_rows))
    placed = butterfly(group_part, own, near_bits, lambda part, bit: from_partner(part, "kv", bit))
    placed = placed.reshape(near, token_count, far, shard_rows).transpose(1, 2, 0, 3)
    partial_out = placed.reshape(token_count, model_width).astype(jnp.float32)
    mixed_out = lax.psum_scatter(
        partial_out.astype(jnp.bfloat16), "tp", scatter_dimension=1, tiled=True
    )
    return mixed_out


def shards(
    tokens,
    norm_gain,
    w_query,
    w_key,
    w_value,
    w_outgate,
    w_gates,
    forget_bias,
    head_gain,
    w_mix,
    state_cell,
    state_norm,
    state_max,
    pend_keys,
    pend_values,
    pend_gates,
    accepted,
):
    sequences, proposals, model_width = tokens.shape
    token_count = sequences * proposals
    local_heads = forget_bias.shape[0]
    head_size = state_cell.shape[-1]
    shard_rows = w_query.shape[0]
    weights = (w_query, w_key, w_value, w_outgate)
    ways, groups = lax.axis_size("kv"), lax.axis_size("tp")
    direct = (
        shard_rows % 256 == 0
        and w_mix.shape[1] == shard_rows
        and w_query.shape[1] == shard_rows
        and ways == 2 * groups
        and groups % 2 == 0
        and sequences == 8
        and head_size == 128
        and token_count <= head_size
    )
    if direct:
        return one_step(
            tokens,
            norm_gain,
            weights,
            w_gates,
            forget_bias,
            head_gain,
            w_mix,
            state_cell,
            state_norm,
            state_max,
            pend_keys,
            pend_values,
            pend_gates,
            accepted,
        )
    flat_gates = w_gates.reshape(shard_rows, -1)
    flat_rows = tokens.reshape(token_count, model_width)
    projected, gate_pre, far_mix = project_by_digits(
        flat_rows, norm_gain, weights + (flat_gates,), w_mix
    )
    queries, new_keys, new_values, outgate = projected
    gate_pre = gate_pre.reshape(sequences, proposals, 2, local_heads)

    def split_heads(array):
        return array.astype(jnp.float32).reshape(sequences, proposals, local_heads, head_size)

    key_scale = head_size ** (-0.5)
    cell_new, norm_new, new_max = fold_pending(
        state_cell,
        state_norm,
        state_max,
        split_heads(pend_keys) * key_scale,
        split_heads(pend_values),
        pend_gates,
        forget_bias,
        accepted,
    )
    log_in = gate_pre[:, :, 0, :]
    log_keep = jax.nn.log_sigmoid(gate_pre[:, :, 1, :] + forget_bias)
    hidden = read_block(
        split_heads(queries),
        split_heads(new_keys) * key_scale,
        split_heads(new_values),
        log_in,
        log_keep,
        cell_new,
        norm_new,
        new_max,
    )
    normed = hidden * lax.rsqrt(jnp.mean(hidden * hidden, axis=-1, keepdims=True) + epsilon)
    normed = normed * head_gain.reshape(local_heads, head_size)
    gated_rows = (jax.nn.sigmoid(split_heads(outgate)) * normed).astype(jnp.bfloat16)
    gated_rows = gated_rows.reshape(token_count, local_heads * head_size)
    mixed_out = mix_by_digits(gated_rows, far_mix, model_width)
    return (mixed_out.reshape(sequences, proposals, -1), cell_new, norm_new, new_max)


def solution(mesh):
    return jax.shard_map(
        shards,
        mesh=mesh,
        in_specs=(
            P("kv", None, None),
            P(),
            P("kv", "tp"),
            P("kv", "tp"),
            P("kv", "tp"),
            P("kv", "tp"),
            P("kv", None, "tp"),
            P("tp"),
            P("tp"),
            P("tp", "kv"),
            P("kv", "tp", None, None),
            P("kv", "tp", None),
            P("kv", "tp"),
            P("kv", None, "tp"),
            P("kv", None, "tp"),
            P("kv", None, None, "tp"),
            P("kv"),
        ),
        out_specs=(
            P("kv", None, "tp"),
            P("kv", "tp", None, None),
            P("kv", "tp", None),
            P("kv", "tp"),
        ),
        check_vma=False,
    )
```

time: 76.9 us -> 58.5 us (0.76)
  matrix products: 5.73 us -> 0 us
  local copies, waits for them, and re-layouts: 10.4 us -> 5.88 us
  Pallas kernels: 56.1 us -> 51.8 us
  other arithmetic: 3.09 us -> 0 us
    dot_general x5 -> x0, matrix products: 5.73 us -> none  [the longest x1 3.7 us: fold_pending(): jnp.einsum('sphd,sphe->shde', weighted_keys, value_rows, precision=highest)]
    pallas_call x2 -> x1, Pallas kernels: 56.2 us -> 51.8 us  [one_step(): pl.pallas_call(functools.partial(step_kernel, ways, groups, seqs), out_sh...]
    reshape x6 -> x0, local copies, waits for them, and re-layouts: 3.23 us -> none  [the longest x1 1.3 us: shards(): flat_gates = w_gates.reshape(shard_rows, -1)]
    unnamed x24 -> x8, local copies, waits for them, and re-layouts: 4.34 us -> 5.88 us
    mul x2 -> x0, other arithmetic: 0.88 us -> none  [the longest x1 0.86 us: shards(): split_heads(new_keys) * key_scale]
    split x1 -> x0, local copies, waits for them, and re-layouts: 0.83 us -> none  [shards(): jnp.split(columns, len(weights), axis=1)]
    reshape x1 -> x0, other arithmetic: 0.81 us -> none  [split_heads(): array.astype(jnp.float32)]
    pallas_call x1 -> x0, local copies, waits for them, and re-layouts: 0.8 us -> none  [project(): pl.pallas_call(functools.partial(project_kernel, ways), out_shape=(jax.Sh...]
where the time goes in v1:
time: 58.5 us; the launch traced here: 58.4 us
  Pallas kernels  51.8 us (89%)
  local copies, waits for them, and re-layouts  5.88 us (10%)
  between operations  0.65 us (1%)
    pallas_call x1, Pallas kernels, one_step(): pl.pallas_call(functools.partial(step_kernel, ways, groups, seqs), out_sh...  51.8 us
    unnamed x8, local copies, waits for them, and re-layouts  5.88 us

profile of v1, /device:TPU:0, one launch (start us, length us, event | category | flops | bytes accessed | tf_op | source)
XLA Modules:
  0.0 58.4 jit_solution(3773541664708668799)
XLA Ops:
  0.6 51.8 %shard_map.192 = (bf16[48,1024]{1,0:T(8,128)(2,1)}, f32[8,4,128,128]{3,2,1,0:T(8,128)}, f32[8,4,128]{2,1,0:T(4,128)}, f32[4,8]{1,0:T(4,128)}) custom-call(bf16[48,4096]{1,0:T(8,128)(2,1)} %bitcast.20, f32[1,4096]{1,0:T(1,128)} %bitcast.25, bf16[512,512]{1,0:T(8,128)(2,1)} %wq_hbm.1, bf16[512,512]{1,0:T(8,128)(2,1)} %wk_hbm.1, bf16[512,512]{1,0:T(8,128)(2,1)} %wv_hbm.1, ...), custom_call_target="tpu_custom_call" | custom-call | tf_op jit(solution)/shard_map/pallas_call | solution.py:795
  52.5 1.5 %copy.25 = bf16[8,6,1024]{2,0,1:T(8,128)(2,1)} copy(bf16[8,6,1024]{2,0,1:T(8,128)(2,1)} %bitcast.21) | data formatting | bytes 196608
  54.0 0.0 copy-start
  54.0 0.0 copy-start.1
  54.0 3.1 %copy.26 = f32[8,4,128,128]{3,2,1,0:T(8,128)} copy(f32[8,4,128,128]{3,2,1,0:T(8,128)} %get-tuple-element.17) | data formatting | bytes 4194304
  57.2 0.0 copy-done
  57.2 0.6 %copy.27 = f32[8,4,128]{2,1,0:T(4,128)} copy(f32[8,4,128]{2,1,0:T(4,128)S(1)} %copy-done) | data formatting | bytes 32768
  57.8 0.0 copy-done.1
  57.8 0.6 copy.28
Async XLA Ops:
  54.0 3.2 %copy-start = (f32[8,4,128]{2,1,0:T(4,128)S(1)}, f32[8,4,128]{2,1,0:T(4,128)}, u32[]{:S(2)}) copy-start(f32[8,4,128]{2,1,0:T(4,128)} %get-tuple-element.18) | copy-start | bytes 49156
  54.0 3.8 %copy-start.1 = (f32[4,8]{1,0:T(4,128)S(1)}, f32[4,8]{1,0:T(4,128)}, u32[]{:S(2)}) copy-start(f32[4,8]{1,0:T(4,128)} %get-tuple-element.11) | copy-start | bytes 388

commit v2 on v1

--- a/solution.py
+++ b/solution.py
@@ -161,10 +161,10 @@
     pend_v_hbm,
     pend_g_hbm,
     accepted_hbm,
-    out_hbm,
-    cell_out_hbm,
-    norm_out_hbm,
-    max_out_hbm,
+    out,
+    cell_new,
+    norm_new,
+    max_new,
     tok,
     gain,
     weights,
@@ -179,10 +179,6 @@
     pend_v,
     pend_g,
     accepted,
-    out,
-    cell_new,
-    norm_new,
-    max_new,
     tok_in,
     scaled,
     wg_in,
@@ -203,7 +199,6 @@
     answer_out,
     answer_in,
     load_sem,
-    store_sem,
     tok_send,
     tok_recv,
     fwd_send,
@@ -425,13 +420,6 @@
         for index, piece in enumerate(pieces):
             fold_rows[index * heads : (index + 1) * heads, 0:seqs] = piece
         return fold_rows[...].T[:seqs]
-
-    stores = []
-
-    def store(source, target_ref):
-        copy = pltpu.make_async_copy(source, target_ref, store_sem.at[len(stores)])
-        copy.start()
-        stores.append(copy)
 
     key_scale = head_size ** (-0.5)
 
@@ -485,9 +473,6 @@
         loads[name].wait()
     for head in range(heads):
         fold_head(cols, head)
-    store(cell_new, cell_out_hbm)
-    store(norm_new, norm_out_hbm)
-    store(max_new, max_out_hbm)
 
     for shift in keepers:
         arrive(shift)
@@ -702,7 +687,6 @@
             term = answer_in[slot].astype(f32)
             total = term if total is None else total + term
         out[:, which * width : (which + 1) * width] = total.astype(bf16)
-    store(out, out_hbm)
     for copy in sends:
         copy.wait_send()
 
@@ -710,7 +694,17 @@
     def _():
         answer(0).wait_send()
 
-    for copy in stores:
+
+def deliver_kernel(*refs):
+    sem = refs[-1]
+    total = len(refs) // 2
+    copies = [
+        pltpu.make_async_copy(refs[index], refs[total + index], sem.at[index])
+        for index in range(total)
+    ]
+    for copy in copies:
+        copy.start()
+    for copy in copies:
         copy.wait()
 
 
@@ -758,15 +752,14 @@
         pend_gates.transpose(1, 2, 3, 0),
         accepted[None, :],
     )
-    out_shape = (
-        jax.ShapeDtypeStruct((count, ways // groups * width), bf16),
-        jax.ShapeDtypeStruct(state_cell.shape, f32),
-        jax.ShapeDtypeStruct(state_norm.shape, f32),
-        jax.ShapeDtypeStruct((heads, seqs), f32),
+    results = (
+        ((count, ways // groups * width), bf16),
+        (state_cell.shape, f32),
+        (state_norm.shape, f32),
+        ((heads, seqs), f32),
     )
     held = [jax.ShapeDtypeStruct(array.shape, array.dtype) for array in operands]
     held = held[:2] + [jax.ShapeDtypeStruct((chunks, rows, 4 * span), bf16)] + held[6:]
-    held = held + list(out_shape)
     block = (ways, count, rows)
     scratch = [pltpu.VMEM(array.shape, array.dtype) for array in held]
     scratch += [
@@ -787,19 +780,30 @@
     ]
     scratch += [pltpu.VMEM((ways // 2, count, width), bf16)] * 5
     dma = pltpu.SemaphoreType.DMA
-    scratch += [dma((len(operands) + 4 * chunks,)), dma((8,))]
+    scratch += [dma((len(operands) + 4 * chunks,))]
     scratch += [dma((ways,))] * 6
     scratch += [dma((chunks, ways))] * 4
     scratch += [dma((ways,))] * 4
-    anywhere = pl.BlockSpec(memory_space=pl.ANY)
+    hbm = pltpu.MemorySpace.HBM
+    anywhere = pl.BlockSpec(memory_space=hbm)
+    vmem = pl.BlockSpec(memory_space=pltpu.VMEM)
+    held = pl.pallas_call(
+        functools.partial(step_kernel, ways, groups, seqs),
+        out_shape=tuple(pltpu.VMEM(shape, dtype) for shape, dtype in results),
+        in_specs=[anywhere] * len(operands),
+        out_specs=(vmem,) * len(results),
+        scratch_shapes=scratch,
+        compiler_params=pltpu.CompilerParams(
+            collective_id=0, has_side_effects=True, vmem_limit_bytes=40 * 2**20
+        ),
+    )(*(pltpu.with_memory_space_constraint(array, hbm) for array in operands))
     mixed_out, cell_new, norm_new, max_new = pl.pallas_call(
-        functools.partial(step_kernel, ways, groups, seqs),
-        out_shape=out_shape,
-        in_specs=[anywhere] * len(operands),
-        out_specs=(anywhere,) * 4,
-        scratch_shapes=scratch,
-        compiler_params=pltpu.CompilerParams(collective_id=0, has_side_effects=True),
-    )(*operands)
+        deliver_kernel,
+        out_shape=tuple(jax.ShapeDtypeStruct(shape, dtype) for shape, dtype in results),
+        in_specs=[vmem] * len(results),
+        out_specs=(anywhere,) * len(results),
+        scratch_shapes=[dma((len(results),))],
+    )(*(pltpu.with_memory_space_constraint(array, pltpu.VMEM) for array in held))
     mixed_out = mixed_out.reshape(proposals, seqs, -1).transpose(1, 0, 2)
     return mixed_out, cell_new, norm_new, max_new.T
 

time: 58.5 us -> 53.4 us (0.913)
  local copies, waits for them, and re-layouts: 5.88 us -> 0 us
  Pallas kernels: 51.8 us -> 52.6 us
    unnamed x8 -> x0, local copies, waits for them, and re-layouts: 5.88 us -> none
    pallas_call x0 -> x1, Pallas kernels: none -> 1.39 us  [one_step(): pl.pallas_call(deliver_kernel, out_shape=tuple((jax.ShapeDtypeStruct(shap...]
    pallas_call x1, Pallas kernels: 51.8 us -> 51.2 us  [one_step(): pl.pallas_call(functools.partial(step_kernel, ways, groups, seqs), out_sh...]
where the time goes in v2:
time: 53.4 us; the launch traced here: 53.3 us
  Pallas kernels  52.6 us (99%)
  between operations  0.65 us (1%)
    pallas_call x1, Pallas kernels, one_step(): pl.pallas_call(functools.partial(step_kernel, ways, groups, seqs), out_sh...  51.2 us
    pallas_call x1, Pallas kernels, one_step(): pl.pallas_call(deliver_kernel, out_shape=tuple((jax.ShapeDtypeStruct(shap...  1.39 us

profile of v2, /device:TPU:0, one launch (start us, length us, event | category | flops | bytes accessed | tf_op | source)
XLA Modules:
  0.0 53.3 jit_solution(17804611993015006355)
XLA Ops:
  0.6 51.2 %shard_map.192 = (bf16[48,1024]{1,0:T(8,128)(2,1)S(1)}, f32[8,4,128,128]{3,2,1,0:T(8,128)S(1)}, f32[8,4,128]{2,1,0:T(4,128)S(1)}, f32[4,8]{1,0:T(4,128)S(1)}) custom-call(bf16[48,4096]{1,0:T(8,128)(2,1)} %bitcast.20, f32[1,4096]{1,0:T(1,128)} %bitcast.24, bf16[512,512]{1,0:T(8,128)(2,1)} %wq_hbm.1, bf16[512,512]{1,0:T(8,128)(2,1)} %wk_hbm.1, ...), custom_call_target="tpu_custom_call" | custom-call | tf_op jit(solution)/shard_map/pallas_call | solution.py:790
  51.9 1.4 %shard_map.193 = (bf16[48,1024]{1,0:T(8,128)(2,1)}, f32[8,4,128,128]{3,2,1,0:T(8,128)}, f32[8,4,128]{2,1,0:T(4,128)}, f32[4,8]{1,0:T(4,128)}) custom-call(bf16[48,1024]{1,0:T(8,128)(2,1)S(1)} %get-tuple-element.12.refs_0_, f32[8,4,128,128]{3,2,1,0:T(8,128)S(1)} %get-tuple-element.13.refs_1_, f32[8,4,128]{2,1,0:T(4,128)S(1)} %get-tuple-element.14.refs_2_, ...), custom_call_target="tpu_custom_call" | custom-call | tf_op jit(solution)/shard_map/pallas_call | solution.py:800

commit v3 on v2

--- a/solution.py
+++ b/solution.py
@@ -138,6 +138,11 @@
             index = index + place * (1 - 2 * (index // place % 2))
         place *= 2
     return index
+
+
+spread_chunks = (3,)
+tasks = (('forward', 3), ('forward', 6), ('gate fold', 0), ('forward', 5), ('forward', 4), ('forward', 7), ('weights', 0), ('arrive', 3), ('send', (3, 0)), ('send', (3, 1)), ('arrive', 6), ('send', (6, 0)), ('arrive', 5), ('send', (5, 1)), ('arrive', 7), ('send', (7, 0)), ('send', (7, 1)), ('send', (7, 2)), ('send', (3, 2)), ('send', (5, 2)), ('send', (7, 3)), ('send', (3, 3)), ('send', (5, 3)), ('arrive', 4), ('sums', 0), ('fold', 0), ('fold', 1), ('fold', 2), ('fold', 3), (0, 0), ('sums', 1), (0, 1), (1, 0), ('sums', 2), (0, 2), (1, 1), ('squares', 0), ('gates', 0), ('sums', 3), (2, 0), (1, 2), (0, 3), (2, 1), ('pass', 0), (2, 2), ('pass', 1), (1, 3), ('pass', 2),
+)
 
 
 def step_kernel(
@@ -193,9 +198,6 @@
     scale_col,
     gated,
     gated_in,
-    swap_out,
-    swap_in,
-    kept,
     answer_out,
     answer_in,
     load_sem,
@@ -209,8 +211,9 @@
     part_recv,
     gated_send,
     gated_recv,
-    swap_send,
-    swap_recv,
+    pass_send,
+    mix_send,
+    mix_recv,
     answer_send,
     answer_recv,
 ):
@@ -227,7 +230,18 @@
     proposals = count // seqs
     bits = ways.bit_length() - 1
     f32, bf16 = jnp.float32, jnp.bfloat16
-    orders = [tuple(range(bits))] * chunks
+    near_first = tuple(range(bits))
+    far_first = near_first[1:] + near_first[:1]
+    plans = [(near_first, False)] * chunks
+    plans[0] = (far_first, False)
+    plans[-1] = (near_first, True)
+
+    def first_bit(chunk):
+        return 1 << plans[chunk][0][0]
+
+    def slot(chunk, shift):
+        return sum(1 for other in range(shift) if not other & first_bit(chunk))
+
 
     loads = {}
 
@@ -255,7 +269,7 @@
     load("norm", norm_hbm, norm)
     load("cell", cell_hbm, cell)
     load("head_gain", head_gain_hbm, head_gain)
-    load("mix", mix_hbm, mix_w)
+    load("mix", mix_hbm, mix_w.at[core])
 
     target = me // 2
     at_home = jnp.logical_and(target == group, core == 0)
@@ -268,7 +282,8 @@
 
     partner = {"tp": 2 * across + 1 - core}
     for shift in range(1, ways):
-        signal({"kv": flipped(me, shift)})
+        for other in range(2):
+            signal({"kv": flipped(me, shift), "tp": 2 * across + other})
     signal(partner)
     for which in range(2):
         sender = 2 * group + which
@@ -280,13 +295,15 @@
             def _():
                 signal({"kv": sender, "tp": sender_group})
 
+    greetings = 2 * (ways - 1) + 1 + ways // 2
+
     @pl.when(at_home)
     def _():
-        pl.semaphore_wait(barrier, ways + ways // 2 - 1)
+        pl.semaphore_wait(barrier, greetings - 1)
 
     @pl.when(jnp.logical_not(at_home))
     def _():
-        pl.semaphore_wait(barrier, ways + ways // 2)
+        pl.semaphore_wait(barrier, greetings)
 
     sends = []
 
@@ -310,11 +327,11 @@
 
     tok_copies, fwd_copies, wg_copies = {}, {}, {}
     loads["tok"].wait()
-    whole_first = 1
+    whole = (1, 2)
 
     def send_tokens(shift):
         there = flipped(me, shift)
-        if shift == whole_first:
+        if shift in whole:
             source, place = tok.at[:, columns(there)], tok_in.at[shift]
         else:
             source = tok.at[:, pl.ds(pl.multiple_of(there * rows + core * half, half), half)]
@@ -323,15 +340,9 @@
             source, place, tok_send.at[shift], tok_recv.at[shift], {"kv": there}
         )
 
-    first_sends = [shift for shift in range(ways - 1, 1, -1) if shift % 2]
-    keepers = [shift for shift in range(ways - 1, 0, -1) if not shift % 2]
-    for shift in [whole_first] + first_sends + keepers:
+    others = [shift for shift in (7, 3, 6, 5, 4) if shift < ways]
+    for shift in list(whole) + others:
         send_tokens(shift)
-    loads["wg"].wait()
-    for shift in range(1, ways):
-        wg_copies[shift] = remote(
-            wg, wg_in.at[shift], wg_send.at[shift], wg_recv.at[shift], {"kv": flipped(me, shift)}
-        )
 
     loads["gain"].wait()
     own_gain = gain[:, columns(me)]
@@ -347,7 +358,7 @@
         )
 
     def arrive(shift):
-        if shift == whole_first:
+        if shift in whole:
             tok_copies[shift].wait_recv()
         else:
             fwd_copies[shift].wait_recv()
@@ -357,37 +368,52 @@
         return jnp.dot(scaled[shift], weights[chunk], preferred_element_type=f32)
 
     part_copies = {}
-
-    def send_part(chunk, shift, bit, value):
+    mix_copy = []
+
+    def send_part(chunk, shift, move, value):
         part_out[chunk, shift] = value.astype(bf16)
         part_copies[chunk, shift] = remote(
             part_out.at[chunk, shift],
             part_in.at[chunk, shift],
             part_send.at[chunk, shift],
             part_recv.at[chunk, shift],
-            {"kv": flipped(me, 1 << bit)},
-        )
-
-    def first_send(chunk, shift):
-        send_part(chunk, shift, orders[chunk][0], product(chunk, shift))
+            {"kv": flipped(me, move)},
+        )
+
+    def first_send(shift, some):
+        for chunk in some:
+            if shift & first_bit(chunk):
+                send_part(chunk, shift, first_bit(chunk), product(chunk, shift))
 
     scale_block(0, tok[:, columns(me)])
-    squares = jnp.zeros((count, 1), f32)
-    for step in range(ways):
-        part = tok[:, step * rows : (step + 1) * rows].astype(f32)
-        squares = squares + jnp.sum(part * part, axis=1, keepdims=True)
-    row_scale = lax.rsqrt(squares / model_width + epsilon)
-    scale_col[...] = jnp.broadcast_to(row_scale, scale_col.shape)
-
     for chunk in range(chunks):
         for index in range(4):
             loads["weight", chunk, index].wait()
 
-    arrive(whole_first)
-    for chunk in range(chunks):
-        first_send(chunk, whole_first)
-    for shift in first_sends:
-        forward(shift)
+    every = range(chunks)
+    for shift in whole:
+        arrive(shift)
+        first_send(shift, every)
+    def send_gates():
+        loads["mix"].wait()
+        mix_copy.append(remote(mix_w.at[core], mix_w.at[core], mix_send, mix_recv, partner))
+        loads["wg"].wait()
+        for shift in range(1, ways):
+            wg_copies[shift] = remote(
+                wg,
+                wg_in.at[shift],
+                wg_send.at[shift],
+                wg_recv.at[shift],
+                {"kv": flipped(me, shift)},
+            )
+
+    def square_rows():
+        squares = jnp.zeros((count, 1), f32)
+        for step in range(ways):
+            part = tok[:, step * rows : (step + 1) * rows].astype(f32)
+            squares = squares + jnp.sum(part * part, axis=1, keepdims=True)
+        row_scale = lax.rsqrt(squares / model_width + epsilon)
+        scale_col[...] = jnp.broadcast_to(row_scale, scale_col.shape)
 
     def eye(size):
         across_rows = lax.broadcasted_iota(jnp.int32, (size, size), 0)
@@ -461,42 +487,30 @@
             cell_high[head, at, :] = upper
             cell_low[head, at, :] = (result - upper.astype(f32)).astype(bf16)
 
-    cols = fold_gates()
-    for shift in first_sends:
-        arrive(shift)
-    for chunk in range(chunks):
-        for shift in first_sends:
-            first_send(chunk, shift)
-    for shift in keepers:
-        forward(shift)
-    for name in ("pend_k", "pend_v", "norm", "cell"):
-        loads[name].wait()
-    for head in range(heads):
-        fold_head(cols, head)
-
-    for shift in keepers:
-        arrive(shift)
-    for chunk in range(chunks):
-        for shift in keepers + [0]:
-            sums[chunk, shift // 2] = product(chunk, shift)
+    cols = []
+
+    def own_sums(chunk):
+        for shift in range(ways):
+            if not shift & first_bit(chunk):
+                sums[chunk, slot(chunk, shift)] = product(chunk, shift)
 
     contract = (((1,), (1,)), ((), ()))
-    gates = [jnp.zeros((count, heads), f32)] * 2
-    for shift in range(ways):
-        owner = flipped(me, shift)
-        if shift:
-            wg_copies[shift].wait_recv()
-            block = (tok[:, columns(owner)].astype(f32) * gain[:, columns(owner)]).astype(bf16)
-        else:
-            block = scaled[0]
-        for part in range(2):
-            right = wg_in[shift, part] if shift else wg[part]
-            gates[part] = gates[part] + lax.dot_general(
-                block, right, contract, preferred_element_type=f32
-            )
 
     def read_gates():
-        stabilizer = cols[:, (proposals + 1) * heads : (proposals + 2) * heads]
+        gates = [jnp.zeros((count, heads), f32)] * 2
+        for shift in range(ways):
+            owner = flipped(me, shift)
+            if shift:
+                wg_copies[shift].wait_recv()
+                block = (tok[:, columns(owner)].astype(f32) * gain[:, columns(owner)]).astype(bf16)
+            else:
+                block = scaled[0]
+            for part in range(2):
+                right = wg_in[shift, part] if shift else wg[part]
+                gates[part] = gates[part] + lax.dot_general(
+                    block, right, contract, preferred_element_type=f32
+                )
+        stabilizer = cols[0][:, (proposals + 1) * heads : (proposals + 2) * heads]
         log_in, running = [], []
         total = jnp.zeros((seqs, heads), f32)
         scale = scale_col[:, :1]
@@ -516,31 +530,74 @@
                 decay[index, :, :heads] = jnp.exp(-top if values is None else values - top)
                 index += 1
 
-    read_gates()
-
-    gated_copies = {}
-
-    def send_gated(chunk, shift, there):
+    first_core, second_core = core == 0, core == 1
+
+    def gated_copy(chunk, source, pair, origin, send_sem, there, there_core):
         place = slice(chunk * span, (chunk + 1) * span)
-        source = gated.at[:, place]
-        gated_copies[chunk, shift] = remote(
-            source,
-            gated_in.at[shift, :, place],
-            gated_send.at[chunk, shift],
-            gated_recv.at[chunk, shift],
-            {"kv": there},
-        )
-
-    def forward_gated(chunk, shift):
+        return pltpu.make_async_remote_copy(
+            src_ref=source.at[:, place],
+            dst_ref=gated_in.at[pair, origin, :, place],
+            send_sem=send_sem,
+            recv_sem=gated_recv.at[chunk, 2 * pair + origin],
+            device_id={"kv": there, "tp": 2 * across + there_core},
+            device_id_type=pl.DeviceIdType.MESH,
+        )
+
+    def to_own_chip(chunk):
+        return gated_copy(chunk, gated, 0, core, gated_send.at[chunk, 0], me, 0)
+
+    def arrived(chunk, pair, origin):
         place = slice(chunk * span, (chunk + 1) * span)
-        gated_copies[chunk, shift].wait_recv()
-        gated_copies[chunk, shift + 1] = remote(
-            gated_in.at[shift, :, place],
-            gated_in.at[shift + 1, :, place],
-            gated_send.at[chunk, shift + 1],
-            gated_recv.at[chunk, shift + 1],
-            {"kv": flipped(me, 1)},
-        )
+        pltpu.make_async_copy(
+            gated.at[:, place],
+            gated_in.at[pair, origin, :, place],
+            gated_recv.at[chunk, 2 * pair + origin],
+        ).wait()
+
+    def passed(chunk, pair, origin):
+        return gated_copy(
+            chunk,
+            gated_in.at[pair, origin],
+            pair,
+            origin,
+            pass_send.at[chunk, 2 * pair + origin],
+            flipped(me, 1),
+            1,
+        )
+
+    def send_gated(chunk):
+        for shift in range(ways - 1, 0, -1):
+            if chunk in spread_chunks or shift == 1 or not shift % 2:
+                copy = gated_copy(
+                    chunk,
+                    gated,
+                    shift // 2,
+                    core,
+                    gated_send.at[chunk, shift],
+                    flipped(me, shift),
+                    shift % 2,
+                )
+                copy.start()
+                sends.append(copy)
+
+        @pl.when(second_core)
+        def _():
+            to_own_chip(chunk).start()
+
+        @pl.when(first_core)
+        def _():
+            place = slice(chunk * span, (chunk + 1) * span)
+            pltpu.make_async_copy(
+                gated.at[:, place], gated_in.at[0, 0, :, place], gated_recv.at[chunk, 0]
+            ).start()
+
+    def pass_gated(chunk):
+        @pl.when(first_core)
+        def _():
+            for pair in range(ways // 2 - 1, 0, -1):
+                for origin in range(2):
+                    arrived(chunk, pair, origin)
+                    passed(chunk, pair, origin).start()
 
     def read_head(chunk, local, flat):
         head = chunk * per_chunk + local
@@ -587,62 +644,65 @@
         normed = normed * head_gain[:, lanes]
         gated[:, lanes] = (jax.nn.sigmoid(outgate) * normed).astype(bf16)
 
+    def complete(chunk, value):
+        for local in range(per_chunk):
+            read_head(chunk, local, value)
+        send_gated(chunk)
+
     def take(chunk, stage):
-        bit = 1 << orders[chunk][stage]
-        done = sum(1 << orders[chunk][early] for early in range(stage + 1))
-        later = [1 << b for b in orders[chunk][stage + 1 :]]
+        order, straight = plans[chunk]
+        if straight and stage:
+            value = sums[chunk, 0]
+            for shift in range(1, ways):
+                if not shift & first_bit(chunk):
+                    part_copies[chunk, shift].wait_recv()
+                    value = value + part_in[chunk, shift].astype(f32)
+            complete(chunk, value)
+            return
+        bit = 1 << order[stage]
+        done = sum(1 << b for b in order[: stage + 1])
+        later = [1 << b for b in order[stage + 1 :]]
         places = [shift for shift in range(ways) if not shift & done]
         places.sort(key=lambda shift: tuple(-(shift // b % 2) for b in later))
         for shift in places:
             part_copies[chunk, shift + bit].wait_recv()
-            value = sums[chunk, shift // 2] + part_in[chunk, shift + bit].astype(f32)
-            if stage + 1 < bits and shift & later[0]:
-                send_part(chunk, shift, orders[chunk][stage + 1], value)
-            elif stage + 1 < bits:
-                sums[chunk, shift // 2] = value
+            value = sums[chunk, slot(chunk, shift)] + part_in[chunk, shift + bit].astype(f32)
+            if straight and shift:
+                send_part(chunk, shift, shift, value)
+            elif later and shift & later[0]:
+                send_part(chunk, shift, later[0], value)
+            elif later:
+                sums[chunk, slot(chunk, shift)] = value
             else:
-                for local in range(per_chunk):
-                    read_head(chunk, local, value)
-
-    loads["head_gain"].wait()
-    loads["mix"].wait()
-    last = chunks - 1
-    for tick in range(chunks + bits):
-        for stage in range(bits):
-            chunk = tick - stage
-            if 0 <= chunk < chunks:
-                take(chunk, stage)
-                if stage == bits - 1:
-                    for shift in range(ways - 1, 0, -1):
-                        if chunk == last or shift == 1 or not shift % 2:
-                            send_gated(chunk, shift, flipped(me, shift))
-        chunk = tick - bits
-        if 0 <= chunk < last:
-            for shift in range(ways - 2, 0, -2):
-                forward_gated(chunk, shift)
-
-    def mixed(block):
-        return jnp.dot(block, mix_w[...], preferred_element_type=f32)
-
-    swap_copies = {}
-    first_core = core == 0
-    pairs = list(range(ways // 2 - 1, -1, -1))
-    for pair in pairs:
-        values = []
-        for shift in (2 * pair, 2 * pair + 1):
-            if shift:
-                for chunk in range(chunks):
-                    gated_copies[chunk, shift].wait_recv() if (
-                        chunk == last or shift % 2
-                    ) else None
-                values.append(mixed(gated_in[shift]))
-            else:
-                values.append(mixed(gated[...]))
-        kept[pair] = jnp.where(first_core, values[0], values[1]).astype(bf16)
-        swap_out[pair] = jnp.where(first_core, values[1], values[0]).astype(bf16)
-        swap_copies[pair] = remote(
-            swap_out.at[pair], swap_in.at[pair], swap_send.at[pair], swap_recv.at[pair], partner
-        )
+                complete(chunk, value)
+
+    for kind, which in tasks:
+        if kind == "forward":
+            forward(which)
+        elif kind == "arrive":
+            arrive(which)
+        elif kind == "send":
+            first_send(which[0], [which[1]])
+        elif kind == "sums":
+            own_sums(which)
+        elif kind == "gate fold":
+            cols.append(fold_gates())
+        elif kind == "fold":
+            if not which:
+                for name in ("pend_k", "pend_v", "norm", "cell"):
+                    loads[name].wait()
+            fold_head(cols[0], which)
+        elif kind == "weights":
+            send_gates()
+        elif kind == "squares":
+            square_rows()
+        elif kind == "gates":
+            loads["head_gain"].wait()
+            read_gates()
+        elif kind == "pass":
+            pass_gated(which)
+        else:
+            take(which, kind)
 
     spot = side * (groups // 2) + across
 
@@ -659,9 +719,23 @@
         )
 
     at_own = pltpu.make_async_copy(answer_out.at[0], answer_in.at[spot], answer_recv.at[spot])
-    for pair in pairs:
-        swap_copies[pair].wait_recv()
-        answer_out[pair] = (kept[pair].astype(f32) + swap_in[pair].astype(f32)).astype(bf16)
+    mix_copy[0].wait_recv()
+    for pair in range(ways // 2):
+        for chunk in range(chunks):
+            for origin in range(2):
+                if chunk in spread_chunks or not pair:
+                    arrived(chunk, pair, origin)
+        for chunk in range(chunks):
+            if chunk not in spread_chunks and pair:
+
+                @pl.when(second_core)
+                def _():
+                    for origin in range(2):
+                        arrived(chunk, pair, origin)
+
+        value = jnp.dot(gated_in[pair, 0], mix_w[0], preferred_element_type=f32)
+        value = value + jnp.dot(gated_in[pair, 1], mix_w[1], preferred_element_type=f32)
+        answer_out[pair] = value.astype(bf16)
         if pair:
             copy = answer(pair)
             copy.start()
@@ -676,7 +750,7 @@
             def _():
                 answer(0).start()
 
-    width = mix_w.shape[1]
+    width = mix_w.shape[2]
     for which in range(2):
         total = None
         for other in range(groups // 2):
@@ -689,6 +763,19 @@
         out[:, which * width : (which + 1) * width] = total.astype(bf16)
     for copy in sends:
         copy.wait_send()
+
+    @pl.when(second_core)
+    def _():
+        for chunk in range(chunks):
+            to_own_chip(chunk).wait_send()
+
+    @pl.when(first_core)
+    def _():
+        for chunk in range(chunks):
+            if chunk not in spread_chunks:
+                for pair in range(1, ways // 2):
+                    for origin in range(2):
+                        passed(chunk, pair, origin).wait_send()
 
     @pl.when(jnp.logical_not(at_home))
     def _():
@@ -760,6 +847,7 @@
     )
     held = [jax.ShapeDtypeStruct(array.shape, array.dtype) for array in operands]
     held = held[:2] + [jax.ShapeDtypeStruct((chunks, rows, 4 * span), bf16)] + held[6:]
+    held[6] = jax.ShapeDtypeStruct((2,) + w_mix.shape, bf16)
     block = (ways, count, rows)
     scratch = [pltpu.VMEM(array.shape, array.dtype) for array in held]
     scratch += [
@@ -776,14 +864,15 @@
         pltpu.VMEM((proposals * (proposals + 5) // 2, seqs, 128), f32),
         pltpu.VMEM((count, head_size), f32),
         pltpu.VMEM((count, width), bf16),
-        pltpu.VMEM((ways, count, width), bf16),
+        pltpu.VMEM((ways // 2, 2, count, width), bf16),
     ]
-    scratch += [pltpu.VMEM((ways // 2, count, width), bf16)] * 5
+    scratch += [pltpu.VMEM((ways // 2, count, width), bf16)] * 2
     dma = pltpu.SemaphoreType.DMA
     scratch += [dma((len(operands) + 4 * chunks,))]
     scratch += [dma((ways,))] * 6
-    scratch += [dma((chunks, ways))] * 4
-    scratch += [dma((ways,))] * 4
+    scratch += [dma((chunks, ways))] * 5
+    scratch += [dma(())] * 2
+    scratch += [dma((ways,))] * 2
     hbm = pltpu.MemorySpace.HBM
     anywhere = pl.BlockSpec(memory_space=hbm)
     vmem = pl.BlockSpec(memory_space=pltpu.VMEM)
@@ -933,7 +1022,7 @@
         and w_mix.shape[1] == shard_rows
         and w_query.shape[1] == shard_rows
         and ways == 2 * groups
-        and groups % 2 == 0
+        and groups == 4
         and sequences == 8
         and head_size == 128
         and token_count <= head_size

time: 53.4 us -> 52.6 us (0.985)
  the two profiles are of different devices: /device:TPU:0 before, /device:TPU:3 now
where the time goes in v3:
time: 52.6 us; the launch traced here: 52.5 us
  Pallas kernels  51.8 us (98%)
  between operations  0.65 us (1%)
    pallas_call x1, Pallas kernels, one_step(): pl.pallas_call(functools.partial(step_kernel, ways, groups, seqs), out_sh...  50.4 us
    pallas_call x1, Pallas kernels, one_step(): pl.pallas_call(deliver_kernel, out_shape=tuple((jax.ShapeDtypeStruct(shap...  1.39 us

profile of v3, /device:TPU:3, one launch (start us, length us, event | category | flops | bytes accessed | tf_op | source)
XLA Modules:
  0.0 52.5 jit_solution(2680087425055913145)
XLA Ops:
  0.6 50.4 %shard_map.192 = (bf16[48,1024]{1,0:T(8,128)(2,1)S(1)}, f32[8,4,128,128]{3,2,1,0:T(8,128)S(1)}, f32[8,4,128]{2,1,0:T(4,128)S(1)}, f32[4,8]{1,0:T(4,128)S(1)}) custom-call(bf16[48,4096]{1,0:T(8,128)(2,1)} %bitcast.20, f32[1,4096]{1,0:T(1,128)} %bitcast.24, bf16[512,512]{1,0:T(8,128)(2,1)} %wq_hbm.1, bf16[512,512]{1,0:T(8,128)(2,1)} %wk_hbm.1, ...), custom_call_target="tpu_custom_call" | custom-call | tf_op jit(solution)/shard_map/pallas_call | solution.py:879
  51.1 1.4 %shard_map.193 = (bf16[48,1024]{1,0:T(8,128)(2,1)}, f32[8,4,128,128]{3,2,1,0:T(8,128)}, f32[8,4,128]{2,1,0:T(4,128)}, f32[4,8]{1,0:T(4,128)}) custom-call(bf16[48,1024]{1,0:T(8,128)(2,1)S(1)} %get-tuple-element.12.refs_0_, f32[8,4,128,128]{3,2,1,0:T(8,128)S(1)} %get-tuple-element.13.refs_1_, f32[8,4,128]{2,1,0:T(4,128)S(1)} %get-tuple-element.14.refs_2_, ...), custom_call_target="tpu_custom_call" | custom-call | tf_op jit(solution)/shard_map/pallas_call | solution.py:889

commit v4 on v3

--- a/solution.py
+++ b/solution.py
@@ -140,8 +140,61 @@
     return index
 
 
-spread_chunks = (3,)
-tasks = (('forward', 3), ('forward', 6), ('gate fold', 0), ('forward', 5), ('forward', 4), ('forward', 7), ('weights', 0), ('arrive', 3), ('send', (3, 0)), ('send', (3, 1)), ('arrive', 6), ('send', (6, 0)), ('arrive', 5), ('send', (5, 1)), ('arrive', 7), ('send', (7, 0)), ('send', (7, 1)), ('send', (7, 2)), ('send', (3, 2)), ('send', (5, 2)), ('send', (7, 3)), ('send', (3, 3)), ('send', (5, 3)), ('arrive', 4), ('sums', 0), ('fold', 0), ('fold', 1), ('fold', 2), ('fold', 3), (0, 0), ('sums', 1), (0, 1), (1, 0), ('sums', 2), (0, 2), (1, 1), ('squares', 0), ('gates', 0), ('sums', 3), (2, 0), (1, 2), (0, 3), (2, 1), ('pass', 0), (2, 2), ('pass', 1), (1, 3), ('pass', 2),
+spread_chunks = (2, 3)
+tasks = (
+    ("forward", 7),
+    ("forward", 3),
+    ("gate fold", 0),
+    ("forward", 6),
+    ("forward", 5),
+    ("forward", 4),
+    ("weights", 0),
+    ("arrive", 7),
+    ("multiply", 7),
+    ("send", (7, 0)),
+    ("send", (7, 1)),
+    ("arrive", 3),
+    ("multiply", 3),
+    ("send", (3, 0)),
+    ("send", (3, 1)),
+    ("arrive", 6),
+    ("multiply", 6),
+    ("send", (6, 0)),
+    ("send", (6, 1)),
+    ("arrive", 5),
+    ("multiply", 5),
+    ("send", (5, 0)),
+    ("send", (5, 1)),
+    ("send", (7, 2)),
+    ("send", (3, 2)),
+    ("send", (5, 2)),
+    ("send", (7, 3)),
+    ("send", (3, 3)),
+    ("send", (5, 3)),
+    ("arrive", 4),
+    ("multiply", 4),
+    ("multiply", 0),
+    ("fold", 0),
+    ("fold", 1),
+    ("fold", 2),
+    ("fold", 3),
+    (0, 0),
+    (0, 1),
+    (1, 0),
+    ("squares", 0),
+    ("gates", 0),
+    (0, 2),
+    (1, 1),
+    (0, 3),
+    (1, 2),
+    (2, 1),
+    (2, 0),
+    (1, 3),
+    (2, 2),
+    ("pass", 1),
+    ("pass", 0),
+    ("mix", 0),
+    ("mix", 1),
 )
 
 
@@ -196,6 +249,8 @@
     norm_head,
     decay,
     scale_col,
+    keys,
+    values,
     gated,
     gated_in,
     answer_out,
@@ -226,8 +281,9 @@
     half = rows // 2
     chunks, span = weights.shape[0], weights.shape[2] // 4
     heads, head_size = norm.shape[1], norm.shape[2]
-    per_chunk = heads // chunks
     proposals = count // seqs
+    cut = count // 2
+    pair_heads = heads // 2
     bits = ways.bit_length() - 1
     f32, bf16 = jnp.float32, jnp.bfloat16
     near_first = tuple(range(bits))
@@ -364,14 +420,13 @@
             fwd_copies[shift].wait_recv()
         scale_block(shift, tok_in[shift])
 
-    def product(chunk, shift):
-        return jnp.dot(scaled[shift], weights[chunk], preferred_element_type=f32)
+    def half_rows(array, part):
+        return array[part * cut : (part + 1) * cut]
 
     part_copies = {}
     mix_copy = []
 
-    def send_part(chunk, shift, move, value):
-        part_out[chunk, shift] = value.astype(bf16)
+    def start_part(chunk, shift, move):
         part_copies[chunk, shift] = remote(
             part_out.at[chunk, shift],
             part_in.at[chunk, shift],
@@ -380,20 +435,39 @@
             {"kv": flipped(me, move)},
         )
 
-    def first_send(shift, some):
-        for chunk in some:
-            if shift & first_bit(chunk):
-                send_part(chunk, shift, first_bit(chunk), product(chunk, shift))
+    def send_part(chunk, shift, move, value):
+        part_out[chunk, shift] = value.astype(bf16)
+        start_part(chunk, shift, move)
+
+    def first_send(chunk, shift):
+        if shift & first_bit(chunk):
+            start_part(chunk, shift, first_bit(chunk))
+
+    def multiply(shift):
+        for pair in range(2):
+            products = [
+                jnp.dot(scaled[shift], weights[head], preferred_element_type=f32)
+                for head in range(pair * pair_heads, (pair + 1) * pair_heads)
+            ]
+            for part in range(2):
+                chunk = 2 * part + pair
+                value = jnp.concatenate([half_rows(each, part) for each in products], axis=0)
+                if shift & first_bit(chunk):
+                    part_out[chunk, shift] = value.astype(bf16)
+                else:
+                    sums[chunk, slot(chunk, shift)] = value
 
     scale_block(0, tok[:, columns(me)])
     for chunk in range(chunks):
         for index in range(4):
             loads["weight", chunk, index].wait()
 
-    every = range(chunks)
     for shift in whole:
         arrive(shift)
-        first_send(shift, every)
+        multiply(shift)
+        for chunk in range(chunks):
+            first_send(chunk, shift)
+
     def send_gates():
         loads["mix"].wait()
         mix_copy.append(remote(mix_w.at[core], mix_w.at[core], mix_send, mix_recv, partner))
@@ -488,11 +562,6 @@
             cell_low[head, at, :] = (result - upper.astype(f32)).astype(bf16)
 
     cols = []
-
-    def own_sums(chunk):
-        for shift in range(ways):
-            if not shift & first_bit(chunk):
-                sums[chunk, slot(chunk, shift)] = product(chunk, shift)
 
     contract = (((1,), (1,)), ((), ()))
 
@@ -533,10 +602,9 @@
     first_core, second_core = core == 0, core == 1
 
     def gated_copy(chunk, source, pair, origin, send_sem, there, there_core):
-        place = slice(chunk * span, (chunk + 1) * span)
         return pltpu.make_async_remote_copy(
-            src_ref=source.at[:, place],
-            dst_ref=gated_in.at[pair, origin, :, place],
+            src_ref=source,
+            dst_ref=gated_in.at[pair, origin, chunk],
             send_sem=send_sem,
             recv_sem=gated_recv.at[chunk, 2 * pair + origin],
             device_id={"kv": there, "tp": 2 * across + there_core},
@@ -544,20 +612,19 @@
         )
 
     def to_own_chip(chunk):
-        return gated_copy(chunk, gated, 0, core, gated_send.at[chunk, 0], me, 0)
+        return gated_copy(chunk, gated.at[chunk], 0, core, gated_send.at[chunk, 0], me, 0)
 
     def arrived(chunk, pair, origin):
-        place = slice(chunk * span, (chunk + 1) * span)
         pltpu.make_async_copy(
-            gated.at[:, place],
-            gated_in.at[pair, origin, :, place],
+            gated.at[chunk],
+            gated_in.at[pair, origin, chunk],
             gated_recv.at[chunk, 2 * pair + origin],
         ).wait()
 
     def passed(chunk, pair, origin):
         return gated_copy(
             chunk,
-            gated_in.at[pair, origin],
+            gated_in.at[pair, origin, chunk],
             pair,
             origin,
             pass_send.at[chunk, 2 * pair + origin],
@@ -570,7 +637,7 @@
             if chunk in spread_chunks or shift == 1 or not shift % 2:
                 copy = gated_copy(
                     chunk,
-                    gated,
+                    gated.at[chunk],
                     shift // 2,
                     core,
                     gated_send.at[chunk, shift],
@@ -586,9 +653,8 @@
 
         @pl.when(first_core)
         def _():
-            place = slice(chunk * span, (chunk + 1) * span)
             pltpu.make_async_copy(
-                gated.at[:, place], gated_in.at[0, 0, :, place], gated_recv.at[chunk, 0]
+                gated.at[chunk], gated_in.at[0, 0, chunk], gated_recv.at[chunk, 0]
             ).start()
 
     def pass_gated(chunk):
@@ -599,16 +665,17 @@
                     arrived(chunk, pair, origin)
                     passed(chunk, pair, origin).start()
 
-    def read_head(chunk, local, flat):
-        head = chunk * per_chunk + local
-        scale = scale_col[...]
+    def read_head(head, part, flat):
+        scale = scale_col[part * cut : (part + 1) * cut]
+        half_steps = proposals // 2
 
         def piece(index):
-            at = index * span + local * head_size
+            at = index * head_size
             return (flat[:, at : at + head_size] * scale).astype(bf16).astype(f32)
 
         query, key, value, outgate = (piece(index) for index in range(4))
-        key = key * key_scale
+        keys[head, part * cut : (part + 1) * cut] = key * key_scale
+        values[head, part * cut : (part + 1) * cut] = value
         sequence = lax.rem(lax.broadcasted_iota(jnp.int32, query.shape, 0), seqs)
         spread = jnp.concatenate(
             [jnp.where(sequence == seq, query, 0.0).astype(bf16) for seq in range(seqs)], axis=1
@@ -617,9 +684,9 @@
         prior = prior + jnp.dot(spread, cell_low[head], preferred_element_type=f32)
         normer = norm_head[head]
         hidden = []
-        index = 0
-        for step in range(proposals):
-            at = slice(step * seqs, (step + 1) * seqs)
+        for step in range(part * half_steps, (part + 1) * half_steps):
+            index = step * (step + 5) // 2
+            at = slice((step - part * half_steps) * seqs, (step - part * half_steps + 1) * seqs)
             now = query[at]
             numerator, denominator = None, None
 
@@ -628,8 +695,9 @@
 
             for past in range(step + 1):
                 before = slice(past * seqs, (past + 1) * seqs)
-                score = jnp.sum(now * key[before], axis=1, keepdims=True) * factor(index + past)
-                term = score * value[before]
+                score = jnp.sum(now * keys[head, before], axis=1, keepdims=True)
+                score = score * factor(index + past)
+                term = score * values[head, before]
                 numerator = term if numerator is None else numerator + term
                 denominator = score if denominator is None else denominator + score
             prior_w = factor(index + step + 1)
@@ -637,16 +705,18 @@
             denominator = denominator + prior_w * jnp.sum(now * normer, axis=1, keepdims=True)
             floor = factor(index + step + 2)
             hidden.append(numerator / jnp.maximum(jnp.abs(denominator), floor))
-            index += step + 3
         hidden = jnp.concatenate(hidden, axis=0)
         normed = hidden * lax.rsqrt(jnp.mean(hidden * hidden, axis=1, keepdims=True) + epsilon)
-        lanes = slice(head * head_size, (head + 1) * head_size)
-        normed = normed * head_gain[:, lanes]
-        gated[:, lanes] = (jax.nn.sigmoid(outgate) * normed).astype(bf16)
+        normed = normed * head_gain[:, head * head_size : (head + 1) * head_size]
+        return jax.nn.sigmoid(outgate) * normed
 
     def complete(chunk, value):
-        for local in range(per_chunk):
-            read_head(chunk, local, value)
+        part, pair = chunk // 2, chunk % 2
+        done = [
+            read_head(pair * pair_heads + local, part, half_rows(value, local))
+            for local in range(pair_heads)
+        ]
+        gated[chunk] = jnp.concatenate(done, axis=0).astype(bf16)
         send_gated(chunk)
 
     def take(chunk, stage):
@@ -676,15 +746,77 @@
             else:
                 complete(chunk, value)
 
+    spot = side * (groups // 2) + across
+
+    def answer(part, pair):
+        owner = flipped(me, 2 * pair) + core * (1 - 2 * side)
+        return pltpu.make_async_remote_copy(
+            src_ref=answer_out.at[part, pair],
+            dst_ref=answer_in.at[part, spot],
+            send_sem=answer_send.at[part, pair],
+            recv_sem=answer_recv.at[part, spot],
+            device_id={"kv": owner, "tp": target},
+            device_id_type=pl.DeviceIdType.MESH,
+        )
+
+    def at_own(part):
+        return pltpu.make_async_copy(
+            answer_out.at[part, 0], answer_in.at[part, spot], answer_recv.at[part, spot]
+        )
+
+    width = mix_w.shape[2]
+    wide = width // 2
+
+    def mix_half(part):
+        ours = (2 * part, 2 * part + 1)
+        for pair in range(ways // 2):
+            for chunk in ours:
+                if chunk in spread_chunks or not pair:
+                    for origin in range(2):
+                        arrived(chunk, pair, origin)
+                else:
+
+                    @pl.when(second_core)
+                    def _():
+                        for origin in range(2):
+                            arrived(chunk, pair, origin)
+
+            value = jnp.zeros((cut, width), f32)
+            for origin in range(2):
+                blocks = [gated_in[pair, origin, chunk].astype(f32) for chunk in ours]
+                left = jnp.concatenate(
+                    [half_rows(block, local) for block in blocks for local in range(2)], axis=1
+                ).astype(bf16)
+                value = value + jnp.dot(left, mix_w[origin], preferred_element_type=f32)
+            stacked = jnp.concatenate([value[:, :wide], value[:, wide:]], axis=0)
+            answer_out[part, pair] = stacked.astype(bf16)
+            if pair:
+                copy = answer(part, pair)
+                copy.start()
+                sends.append(copy)
+            else:
+
+                @pl.when(at_home)
+                def _():
+                    at_own(part).start()
+
+                @pl.when(jnp.logical_not(at_home))
+                def _():
+                    answer(part, 0).start()
+
     for kind, which in tasks:
         if kind == "forward":
             forward(which)
         elif kind == "arrive":
             arrive(which)
         elif kind == "send":
-            first_send(which[0], [which[1]])
-        elif kind == "sums":
-            own_sums(which)
+            first_send(which[1], which[0])
+        elif kind == "multiply":
+            multiply(which)
+        elif kind == "mix":
+            if not which:
+                mix_copy[0].wait_recv()
+            mix_half(which)
         elif kind == "gate fold":
             cols.append(fold_gates())
         elif kind == "fold":
@@ -704,63 +836,24 @@
         else:
             take(which, kind)
 
-    spot = side * (groups // 2) + across
-
-    def answer(pair):
-        base = flipped(me, 2 * pair)
-        owner = base + core * (1 - 2 * side)
-        return pltpu.make_async_remote_copy(
-            src_ref=answer_out.at[pair],
-            dst_ref=answer_in.at[spot],
-            send_sem=answer_send.at[pair],
-            recv_sem=answer_recv.at[spot],
-            device_id={"kv": owner, "tp": target},
-            device_id_type=pl.DeviceIdType.MESH,
-        )
-
-    at_own = pltpu.make_async_copy(answer_out.at[0], answer_in.at[spot], answer_recv.at[spot])
-    mix_copy[0].wait_recv()
-    for pair in range(ways // 2):
-        for chunk in range(chunks):
-            for origin in range(2):
-                if chunk in spread_chunks or not pair:
-                    arrived(chunk, pair, origin)
-        for chunk in range(chunks):
-            if chunk not in spread_chunks and pair:
-
-                @pl.when(second_core)
-                def _():
-                    for origin in range(2):
-                        arrived(chunk, pair, origin)
-
-        value = jnp.dot(gated_in[pair, 0], mix_w[0], preferred_element_type=f32)
-        value = value + jnp.dot(gated_in[pair, 1], mix_w[1], preferred_element_type=f32)
-        answer_out[pair] = value.astype(bf16)
-        if pair:
-            copy = answer(pair)
-            copy.start()
-            sends.append(copy)
-        else:
-
-            @pl.when(at_home)
-            def _():
-                at_own.start()
-
-            @pl.when(jnp.logical_not(at_home))
-            def _():
-                answer(0).start()
-
-    width = mix_w.shape[2]
     for which in range(2):
-        total = None
-        for other in range(groups // 2):
-            slot = which * (groups // 2) + other
-            pltpu.make_async_copy(
-                answer_out.at[0], answer_in.at[slot], answer_recv.at[slot]
-            ).wait()
-            term = answer_in[slot].astype(f32)
-            total = term if total is None else total + term
-        out[:, which * width : (which + 1) * width] = total.astype(bf16)
+        totals = []
+        for part in range(2):
+            total = None
+            for other in range(groups // 2):
+                spot_at = which * (groups // 2) + other
+                pltpu.make_async_copy(
+                    answer_out.at[part, 0],
+                    answer_in.at[part, spot_at],
+                    answer_recv.at[part, spot_at],
+                ).wait()
+                term = answer_in[part, spot_at].astype(f32)
+                total = term if total is None else total + term
+            totals.append(total)
+        for side_cols in range(2):
+            both = jnp.concatenate([half_rows(total, side_cols) for total in totals], axis=0)
+            at = which * width + side_cols * wide
+            out[:, at : at + wide] = both.astype(bf16)
     for copy in sends:
         copy.wait_send()
 
@@ -779,7 +872,8 @@
 
     @pl.when(jnp.logical_not(at_home))
     def _():
-        answer(0).wait_send()
+        for part in range(2):
+            answer(part, 0).wait_send()
 
 
 def deliver_kernel(*refs):
@@ -863,16 +957,18 @@
         pltpu.VMEM((heads, seqs, head_size), f32),
         pltpu.VMEM((proposals * (proposals + 5) // 2, seqs, 128), f32),
         pltpu.VMEM((count, head_size), f32),
-        pltpu.VMEM((count, width), bf16),
-        pltpu.VMEM((ways // 2, 2, count, width), bf16),
+        pltpu.VMEM((heads, count, head_size), f32),
+        pltpu.VMEM((heads, count, head_size), f32),
+        pltpu.VMEM((chunks, count, span), bf16),
+        pltpu.VMEM((ways // 2, 2, chunks, count, span), bf16),
     ]
-    scratch += [pltpu.VMEM((ways // 2, count, width), bf16)] * 2
+    scratch += [pltpu.VMEM((2, ways // 2, count, width // 2), bf16)] * 2
     dma = pltpu.SemaphoreType.DMA
     scratch += [dma((len(operands) + 4 * chunks,))]
     scratch += [dma((ways,))] * 6
     scratch += [dma((chunks, ways))] * 5
     scratch += [dma(())] * 2
-    scratch += [dma((ways,))] * 2
+    scratch += [dma((2, ways // 2))] * 2
     hbm = pltpu.MemorySpace.HBM
     anywhere = pl.BlockSpec(memory_space=hbm)
     vmem = pl.BlockSpec(memory_space=pltpu.VMEM)
@@ -1023,6 +1119,8 @@
         and w_query.shape[1] == shard_rows
         and ways == 2 * groups
         and groups == 4
+        and local_heads == 4
+        and proposals % 2 == 0
         and sequences == 8
         and head_size == 128
         and token_count <= head_size

time: 52.6 us -> 49.9 us (0.949)
  the two profiles are of different devices: /device:TPU:3 before, /device:TPU:0 now
where the time goes in v4:
time: 49.9 us; the launch traced here: 49.8 us
  Pallas kernels  49.1 us (98%)
  between operations  0.65 us (1%)
    pallas_call x1, Pallas kernels, one_step(): pl.pallas_call(functools.partial(step_kernel, ways, groups, seqs), out_sh...  47.7 us
    pallas_call x1, Pallas kernels, one_step(): pl.pallas_call(deliver_kernel, out_shape=tuple((jax.ShapeDtypeStruct(shap...  1.39 us

profile of v4, /device:TPU:0, one launch (start us, length us, event | category | flops | bytes accessed | tf_op | source)
XLA Modules:
  0.0 49.8 jit_solution(10304347487829924310)
XLA Ops:
  0.6 47.7 %shard_map.192 = (bf16[48,1024]{1,0:T(8,128)(2,1)S(1)}, f32[8,4,128,128]{3,2,1,0:T(8,128)S(1)}, f32[8,4,128]{2,1,0:T(4,128)S(1)}, f32[4,8]{1,0:T(4,128)S(1)}) custom-call(bf16[48,4096]{1,0:T(8,128)(2,1)} %bitcast.20, f32[1,4096]{1,0:T(1,128)} %bitcast.24, bf16[512,512]{1,0:T(8,128)(2,1)} %wq_hbm.1, bf16[512,512]{1,0:T(8,128)(2,1)} %wk_hbm.1, ...), custom_call_target="tpu_custom_call" | custom-call | tf_op jit(solution)/shard_map/pallas_call | solution.py:975
  48.4 1.4 %shard_map.193 = (bf16[48,1024]{1,0:T(8,128)(2,1)}, f32[8,4,128,128]{3,2,1,0:T(8,128)}, f32[8,4,128]{2,1,0:T(4,128)}, f32[4,8]{1,0:T(4,128)}) custom-call(bf16[48,1024]{1,0:T(8,128)(2,1)S(1)} %get-tuple-element.12.refs_0_, f32[8,4,128,128]{3,2,1,0:T(8,128)S(1)} %get-tuple-element.13.refs_1_, f32[8,4,128]{2,1,0:T(4,128)S(1)} %get-tuple-element.14.refs_2_, ...), custom_call_target="tpu_custom_call" | custom-call | tf_op jit(solution)/shard_map/pallas_call | solution.py:985
